TPU v7x, 32 devices: a whole 2x2x4 slice. The times are simulated.
32 devices in a mesh: sp: 8 (over z, y), tp: 4 (over x, core).
Axes of the slice: x: 2, y: 2, z: 4, core: 2. Of those that a mesh axis runs over, the one named last changes fastest.
Arguments:
- tokens: bfloat16 [1280, 2048], P('sp'), may hold values from -6 to 6
- input_gain: float32 [2048], replicated, may hold values from 0.1 to 1.9
- chain_query: bfloat16 [2048, 1024], P('sp', 'tp'), may hold values from -0.125 to 0.125
- forward_gate: bfloat16 [2048, 1024], P('sp', 'tp'), may hold values from -0.125 to 0.125
- backward_gate: bfloat16 [2048, 1024], P('sp', 'tp'), may hold values from -0.125 to 0.125
- chain_value: bfloat16 [2048, 1024], P('sp', 'tp'), may hold values from -0.125 to 0.125
- output_gate: bfloat16 [2048, 1024], P('sp', 'tp'), may hold values from -0.125 to 0.125
- forget_rate: float32 [2, 1024], P(None, 'tp'), may hold values from 0.2 to 6
- chain_gain: float32 [1024], P('tp'), may hold values from 0.1 to 1.9
- query_down: bfloat16 [2048, 768], P('sp'), may hold values from -0.125 to 0.125
- latent_down: bfloat16 [2048, 512], P('sp'), may hold values from -0.125 to 0.125
- rotary_down: bfloat16 [2048, 64], replicated, may hold values from -0.125 to 0.125
- query_latent_gain: float32 [768], replicated, may hold values from 0.1 to 1.9
- latent_gain: float32 [512], replicated, may hold values from 0.1 to 1.9
- query_up: bfloat16 [768, 1536], P(None, 'tp'), may hold values from -0.21875 to 0.21875
- latent_up: bfloat16 [512, 2048], P(None, 'tp'), may hold values from -0.25 to 0.25
- query_head_gain: float32 [192], replicated, may hold values from 0.1 to 1.9
- key_head_gain: float32 [192], replicated, may hold values from 0.1 to 1.9
- mixer_gain: float32 [1024], P('tp'), may hold values from 0.1 to 1.9
- chain_out: bfloat16 [1024, 2048], P('tp', 'sp'), may hold values from -0.125 to 0.125
- attend_out: bfloat16 [1024, 2048], P('tp', 'sp'), may hold values from -0.125 to 0.125
Outputs:
- mixed: float32 [1280, 2048], P(('sp', 'tp'))
All inputs are finite; a program needn't handle non-finite values.
Results may differ from a plain program's by a relative error of at most 0.017.
Values may be sent and summed in bfloat16 or wider, within the bound.
A program may use at most 128 MiB of HBM per device.

v0:
```python
import functools

import jax
import jax.numpy as jnp
import numpy as np
from jax import lax
from jax.experimental import pallas as pl
from jax.experimental.pallas import tpu as pltpu
from jax.sharding import PartitionSpec as P

KEY_DIM = 128
VAL_DIM = 128
NOPE_DIM = 128
ROPE_DIM = 64
VHEAD_DIM = 128
ATT_QK = 192

norm_eps = 1e-06
rope_theta = 10000.0
MESH = pl.DeviceIdType.MESH
VMEM_LIMIT = 60 * 1024 * 1024
f32 = jnp.float32
bf16 = jnp.bfloat16


def greet(peers):
    barrier = pltpu.get_barrier_semaphore()
    for peer in peers:
        pl.semaphore_signal(barrier, inc=1, device_id=peer, device_id_type=MESH)
    pl.semaphore_wait(barrier, len(peers))


def line_and_pair(n):
    me = lax.axis_index("sp")
    lines = n // 2
    outer, inner = me // 2, lax.rem(me, 2)
    partner = {"sp": outer * 2 + 1 - inner}

    def line_peer(d):
        return {"sp": lax.rem(outer + d, lines) * 2 + inner}

    return me, lines, outer, inner, partner, line_peer


def project_kernel(n, count, *refs):
    tokens_ref, gain_ref, rate_ref = refs[:3]
    weights = refs[3 : 3 + count]
    (
        v_ref,
        gate_ref,
        ql_ref,
        ll_ref,
        fq_ref,
        fk_ref,
        bq_ref,
        bk_ref,
        log_ref,
        f_state_ref,
        b_state_ref,
    ) = refs[3 + count : 14 + count]
    rest = refs[14 + count :]
    x_ref, x_recv = rest[0], rest[1]
    w_recv = rest[2 : 2 + count]
    p_send = rest[2 + count : 2 + 2 * count]
    p_recv = rest[2 + 2 * count : 2 + 3 * count]
    own = rest[2 + 3 * count : 2 + 4 * count]
    xs, xr, ws, wr, ps, pr = rest[2 + 4 * count :]
    groups = n // 4
    me = lax.axis_index("sp")
    group, place = me // 4, lax.rem(me, 4)
    low, inner = place // 2, lax.rem(place, 2)
    places = (
        place,
        (1 - low) * 2 + inner,
        low * 2 + 1 - inner,
        (1 - low) * 2 + 1 - inner,
    )
    beside = {"sp": group * 4 + places[1]}
    partner = {"sp": group * 4 + places[2]}

    def far_peer(d):
        return {"sp": lax.rem(group + d, groups) * 4 + place}

    greet([beside, partner] + [far_peer(d) for d in range(1, groups)])

    def w_copy(c, k):
        return pltpu.make_async_remote_copy(
            src_ref=w_recv[c].at[0] if k == 2 else weights[c],
            dst_ref=w_recv[c].at[k],
            send_sem=ws.at[c, k],
            recv_sem=wr.at[c, k],
            device_id=beside if k == 0 else partner,
            device_id_type=MESH,
        )

    def x_copy(d):
        return pltpu.make_async_remote_copy(
            src_ref=x_ref.at[lax.rem(group + d, groups)],
            dst_ref=x_recv.at[d],
            send_sem=xs.at[d],
            recv_sem=xr.at[d],
            device_id=far_peer(d),
            device_id_type=MESH,
        )

    def p_copy(c, d):
        return pltpu.make_async_remote_copy(
            src_ref=p_send[c].at[d],
            dst_ref=p_recv[c].at[d],
            send_sem=ps.at[c, d],
            recv_sem=pr.at[c, d],
            device_id=far_peer(d),
            device_id_type=MESH,
        )

    w_copy(0, 0).start()
    w_copy(0, 1).start()
    wide = tokens_ref[...].astype(f32)
    scale = lax.rsqrt(jnp.mean(wide * wide, axis=-1, keepdims=True) + norm_eps)
    normed = (wide * scale * gain_ref[...]).astype(bf16)
    rows, depth = x_ref.shape[2:]
    for g in range(groups):
        for k in range(4):
            first = (g * 4 + k) * depth
            x_ref[g, k] = normed[:, first : first + depth]
    for d in range(1, groups):
        x_copy(d).start()
    for c in range(1, count):
        w_copy(c, 0).start()
    for c in range(count):
        w_copy(c, 0).wait_recv()
        w_copy(c, 2).start()
        if c + 1 < count:
            w_copy(c + 1, 1).start()
    def finished(c):
        def add(d, total):
            p_copy(c, d).wait_recv()
            return total + p_recv[c][d].astype(f32)

        return lax.fori_loop(1, groups, add, own[c][...]).astype(bf16)

    def recurrence():
        value = finished(0)
        v_ref[...] = value
        row = lax.broadcasted_iota(jnp.int32, (rows, rows), 0)
        col = lax.broadcasted_iota(jnp.int32, (rows, rows), 1)

        def direction(c, mask, last):
            rate = rate_ref[c - 1 : c, :] / (rows * n)
            key = rate * jax.nn.sigmoid(-finished(c).astype(f32))
            total = jnp.dot(
                jnp.where(mask, 1.0, 0.0),
                jnp.log1p(-key),
                precision=lax.Precision.HIGHEST,
                preferred_element_type=f32,
            )
            full = total[last : last + 1, :]
            key = (key * jnp.exp(-total)).astype(bf16)
            state = jnp.concatenate(
                [
                    lax.dot_general(
                        value[:, h * VAL_DIM : (h + 1) * VAL_DIM],
                        key[:, h * KEY_DIM : (h + 1) * KEY_DIM],
                        (((0,), (0,)), ((), ())),
                        preferred_element_type=f32,
                    )
                    for h in range(value.shape[1] // VAL_DIM)
                ],
                axis=1,
            )
            log_ref[c - 1 : c, :] = full
            return key, total, (state * jnp.exp(full)).astype(bf16)

        fk_ref[...], f_total, f_state_ref[...] = direction(1, row >= col, rows - 1)
        bk_ref[...], b_total, b_state_ref[...] = direction(2, row <= col, 0)
        query = finished(3).astype(f32)
        fq_ref[...] = (query * jnp.exp(f_total)).astype(bf16)
        bq_ref[...] = (query * jnp.exp(b_total)).astype(bf16)

    for c in range(count):
        w_copy(c, 1).wait_recv()
        w_copy(c, 2).wait_recv()

        def part(x):
            total = jnp.dot(x(places[0]), weights[c][...], preferred_element_type=f32)
            for k in range(3):
                total += jnp.dot(x(places[k + 1]), w_recv[c][k], preferred_element_type=f32)
            return total

        @pl.loop(1, groups)
        def _(d):
            if c == 0:
                x_copy(d).wait_recv()
            back = groups - d
            p_send[c][back] = part(lambda k: x_recv[d, k]).astype(bf16)
            p_copy(c, back).start()

        own[c][...] = part(lambda k: x_ref[group, k])
        if c == count - 2:
            recurrence()
    gate_ref[...] = finished(4)
    ql_ref[...] = finished(5)
    ll_ref[...] = finished(6)
    for d in range(1, groups):
        x_copy(d).wait_send()
    for c in range(count):
        for k in range(3):
            w_copy(c, k).wait_send()

        @pl.loop(1, groups)
        def _(d):
            p_copy(c, d).wait_send()


def project_all(n, tokens, gain, rates, weights):
    groups = n // 4
    rows, depth = tokens.shape[0], weights[0].shape[0]
    count = len(weights)
    widths = [w.shape[1] for w in weights]
    width = widths[0]
    wide = jax.ShapeDtypeStruct((rows, width), bf16)
    state = jax.ShapeDtypeStruct((VAL_DIM, width), bf16)
    vmem = pl.BlockSpec(memory_space=pltpu.VMEM)
    return pl.pallas_call(
        functools.partial(project_kernel, n, count),
        out_shape=[jax.ShapeDtypeStruct((rows, widths[c]), bf16) for c in (0, 4, 5, 6)]
        + [wide] * 4
        + [jax.ShapeDtypeStruct((2, width), f32), state, state],
        in_specs=[vmem] * (3 + count),
        out_specs=[vmem] * 11,
        scratch_shapes=[pltpu.VMEM((groups, 4, rows, depth), bf16)] * 2
        + [pltpu.VMEM((3, depth, c), bf16) for c in widths]
        + [pltpu.VMEM((groups, rows, c), bf16) for c in widths]
        + [pltpu.VMEM((groups, rows, c), bf16) for c in widths]
        + [pltpu.VMEM((rows, c), f32) for c in widths]
        + [
            pltpu.SemaphoreType.DMA((groups,)),
            pltpu.SemaphoreType.DMA((groups,)),
            pltpu.SemaphoreType.DMA((count, 3)),
            pltpu.SemaphoreType.DMA((count, 3)),
            pltpu.SemaphoreType.DMA((count, groups)),
            pltpu.SemaphoreType.DMA((count, groups)),
        ],
        compiler_params=pltpu.CompilerParams(
            collective_id=0, has_side_effects=True, vmem_limit_bytes=VMEM_LIMIT
        ),
    )(tokens, gain, rates, *weights)


def heads_peer(n, d):
    return {"tp": lax.rem(lax.axis_index("tp") + d, n)}


def mixer_kernel(n, heads_n, *refs):
    count = 5
    query_in, pair_in, ins = refs[0], refs[1], refs[2 : 2 + count]
    (
        fq_ref,
        fk_ref,
        bq_ref,
        bk_ref,
        v_ref,
        gate_ref,
        chain_gain_ref,
        query_latent_gain_ref,
        latent_gain_ref,
        query_up_ref,
        latent_up_ref,
        query_gain_ref,
        key_gain_ref,
        mixer_gain_ref,
        query_tail_ref,
        key_tail_ref,
        cos_ref,
        sin_ref,
        pick_key_ref,
        swap_key_ref,
        pick_plain_ref,
        pick_query_ref,
        swap_query_ref,
        out_ref,
    ) = refs[2 + count : 26 + count]
    rest = refs[26 + count :]
    query_out, pair_out, outs = rest[0], rest[1], rest[2 : 2 + count]
    numer, denom, send, recv, keep, s1, r1, s2, r2, hs1, hr1, hs2, hr2, ss, rs = rest[2 + count :]
    me, lines, outer, inner, partner, line_peer = line_and_pair(n)
    head = lax.axis_index("tp")
    head_lines = heads_n // 2
    head_outer, head_inner = head // 2, lax.rem(head, 2)
    head_partner = {"tp": head_outer * 2 + 1 - head_inner}

    def head_peer(d):
        return {"tp": lax.rem(head_outer + d, head_lines) * 2 + head_inner}

    greet(
        [partner]
        + [line_peer(d) for d in range(1, lines)]
        + [heads_peer(heads_n, d) for d in range(1, heads_n)]
    )
    src = (pair_in,) + tuple(ins)

    def slot(k, at):
        return pair_out.at[head, at] if k == 0 else outs[k - 1].at[at]

    def along(k, d):
        return pltpu.make_async_remote_copy(
            src_ref=src[k],
            dst_ref=slot(k, me),
            send_sem=s1.at[k, d],
            recv_sem=r1.at[k, d],
            device_id=line_peer(d),
            device_id_type=MESH,
        )

    def across(k, d):
        at = lax.rem(outer - d + lines, lines) * 2 + inner
        return pltpu.make_async_remote_copy(
            src_ref=src[k] if isinstance(d, int) and d == 0 else slot(k, at),
            dst_ref=slot(k, at),
            send_sem=s2.at[k, d],
            recv_sem=r2.at[k, d],
            device_id=partner,
            device_id_type=MESH,
        )

    def local(k):
        return pltpu.make_async_copy(src[k], slot(k, me), keep.at[k])

    def head_along(j, d):
        return pltpu.make_async_remote_copy(
            src_ref=query_in if j == 0 else pair_out.at[head],
            dst_ref=query_out.at[head] if j == 0 else pair_out.at[head],
            send_sem=hs1.at[j, d],
            recv_sem=hr1.at[j, d],
            device_id=head_peer(d),
            device_id_type=MESH,
        )

    def head_across(j, d):
        at = lax.rem(head_outer - d + head_lines, head_lines) * 2 + head_inner
        own = isinstance(d, int) and d == 0
        out = query_out if j == 0 else pair_out
        return pltpu.make_async_remote_copy(
            src_ref=query_in if j == 0 and own else out.at[at],
            dst_ref=out.at[at],
            send_sem=hs2.at[j, d],
            recv_sem=hr2.at[j, d],
            device_id=head_partner,
            device_id_type=MESH,
        )

    query_local = pltpu.make_async_copy(query_in, query_out.at[head], keep.at[1 + count])

    def needed(k, there):
        if k == 2:
            return there
        if k == 3:
            return jnp.logical_not(there)
        return None

    def maybe(condition, act):
        if condition is None:
            act()
        else:
            pl.when(condition)(act)

    def on_line(k, sending, act):
        @pl.loop(1, lines)
        def _(d):
            there = outer + d < lines if sending else outer >= d
            maybe(needed(k, there), lambda: act(d))

    for k in range(1 + count):
        on_line(k, True, lambda d: along(k, d).start())
        across(k, 0).start()
        local(k).start()
        if k == 0:
            for d in range(1, head_lines):
                head_along(0, d).start()
            head_across(0, 0).start()
            query_local.start()

    def pass_on(k):
        def act(d):
            along(k, d).wait_recv()
            across(k, d).start()

        on_line(k, False, act)

    pass_on(0)
    for d in range(1, head_lines):
        head_along(0, d).wait_recv()
        head_across(0, d).start()
    local(0).wait()
    across(0, 0).wait_recv()
    on_line(0, False, lambda d: across(0, d).wait_recv())
    for d in range(1, head_lines):
        head_along(1, d).start()
    head_across(1, 0).start()
    for k in range(1, count - 1):
        pass_on(k)

    rows, width = v_ref.shape
    chain_heads = width // KEY_DIM

    def lanes(h, size):
        return slice(h * size, (h + 1) * size)

    def against(a, b):
        return lax.dot_general(a, b, (((1,), (1,)), ((), ())), preferred_element_type=f32)

    row = lax.broadcasted_iota(jnp.int32, (rows, rows), 0)
    col = lax.broadcasted_iota(jnp.int32, (rows, rows), 1)
    within = []
    for h in range(chain_heads):
        at = lanes(h, KEY_DIM)
        both = jnp.where(row >= col, against(fq_ref[:, at], fk_ref[:, at]), 0.0) + jnp.where(
            row <= col, against(bq_ref[:, at], bk_ref[:, at]), 0.0
        )
        within.append(
            jnp.dot(both.astype(bf16), v_ref[:, lanes(h, VAL_DIM)], preferred_element_type=f32)
        )

    for d in range(1, head_lines):
        head_along(1, d).wait_recv()
        head_across(1, d).start()
    for k in (1, 2, 3):
        local(k).wait()
        across(k, 0).wait_recv()
        on_line(k, False, lambda d: across(k, d).wait_recv())

    log_ref, f_ref, b_ref = outs[0], outs[1], outs[2]

    def forward(i, state):
        return state * jnp.exp(log_ref[i, 0:1, :]) + f_ref[i].astype(f32)

    def backward(i, state):
        at = n - 1 - i
        return state * jnp.exp(log_ref[at, 1:2, :]) + b_ref[at].astype(f32)

    nothing = jnp.zeros(f_ref.shape[1:], f32)
    f_in = lax.fori_loop(0, me, forward, nothing).astype(bf16)
    b_in = lax.fori_loop(0, n - 1 - me, backward, nothing).astype(bf16)

    def normed(values, size):
        return lax.rsqrt(jnp.sum(values * values, axis=-1, keepdims=True) / size + norm_eps)

    chain_parts = []
    for h in range(chain_heads):
        at = lanes(h, KEY_DIM)
        total = (
            within[h] + against(fq_ref[:, at], f_in[:, at]) + against(bq_ref[:, at], b_in[:, at])
        )
        gate = gate_ref[:, lanes(h, VAL_DIM)].astype(f32)
        scaled = total * normed(total, VAL_DIM) * chain_gain_ref[:, lanes(h, VAL_DIM)]
        chain_parts.append((scaled * (gate * jax.nn.sigmoid(gate))).astype(bf16))
    chain_mixed = jnp.concatenate(chain_parts, axis=1)
    pass_on(4)

    query_local.wait()
    for j in range(head_lines):
        head_across(0, j).wait_recv()
    raws = [query_out[t].astype(f32) for t in range(heads_n)]
    q_cols = raws[0].shape[1]
    square = sum(jnp.sum(r * r, axis=-1, keepdims=True) for r in raws)
    scale = lax.rsqrt(square / (heads_n * q_cols) + norm_eps)
    attend_q = sum(
        jnp.dot(
            (raws[t] * scale * query_latent_gain_ref[t]).astype(bf16),
            query_up_ref[lanes(t, q_cols), :],
            preferred_element_type=f32,
        )
        for t in range(heads_n)
    ).astype(bf16)
    heads = pick_plain_ref.shape[0]
    query_cos = cos_ref[me] * query_tail_ref[0:1, :]
    query_sin = sin_ref[me] * query_tail_ref[1:2, :]
    q_plain, q_turned = [], []
    for h in range(heads):
        plain = jnp.dot(attend_q, pick_plain_ref[h], preferred_element_type=f32)
        tail = jnp.dot(attend_q, pick_query_ref[h], preferred_element_type=f32)
        swapped = jnp.dot(attend_q, swap_query_ref[h], preferred_element_type=f32)
        square = jnp.sum(plain * plain, axis=-1, keepdims=True) + jnp.sum(
            tail * tail, axis=-1, keepdims=True
        )
        scale = lax.rsqrt(square / ATT_QK + norm_eps)
        q_plain.append((plain * scale * query_gain_ref[...]).astype(bf16))
        q_turned.append(
            ((tail * query_cos + swapped * query_sin) * scale).astype(bf16)
        )

    for d in range(head_lines):
        head_across(1, d).wait_recv()
    numer[...] = jnp.zeros_like(numer)
    denom[...] = jnp.zeros_like(denom)
    l_cols = latent_up_ref.shape[0] // heads_n

    def attend(at, carry):
        pieces = [pair_out[t, at] for t in range(heads_n)]
        wide = [p[:, :l_cols].astype(f32) for p in pieces]
        square = sum(jnp.sum(w * w, axis=-1, keepdims=True) for w in wide)
        scale = lax.rsqrt(square / (heads_n * l_cols) + norm_eps)
        latent = jnp.concatenate(
            [
                (wide[t] * scale * latent_gain_ref[:, lanes(t, l_cols)]).astype(bf16)
                for t in range(heads_n)
            ],
            axis=1,
        )
        pairs = jnp.dot(latent, latent_up_ref[...], preferred_element_type=f32).astype(bf16)
        tail = sum(
            jnp.dot(pieces[t], pick_key_ref[t], preferred_element_type=f32)
            for t in range(heads_n)
        )
        swapped = sum(
            jnp.dot(pieces[t], swap_key_ref[t], preferred_element_type=f32)
            for t in range(heads_n)
        )
        tail_square = jnp.sum(tail * tail, axis=-1, keepdims=True)
        turned = (tail * key_tail_ref[0:1, :]) * cos_ref[at] + (
            swapped * key_tail_ref[1:2, :]
        ) * sin_ref[at]
        for h in range(heads):
            start = h * (NOPE_DIM + VHEAD_DIM)
            plain = pairs[:, start : start + NOPE_DIM].astype(f32)
            value = pairs[:, start + NOPE_DIM : start + NOPE_DIM + VHEAD_DIM]
            square = jnp.sum(plain * plain, axis=-1, keepdims=True) + tail_square
            scale = lax.rsqrt(square / ATT_QK + norm_eps)
            score = against(
                q_plain[h], (plain * scale * key_gain_ref[...]).astype(bf16)
            ) + against(q_turned[h], (turned * scale).astype(bf16))
            weight = jnp.exp(score * ATT_QK ** (-0.5))
            numer[h] += jnp.dot(weight.astype(bf16), value, preferred_element_type=f32)
            denom[h] += jnp.sum(weight, axis=-1, keepdims=True)
        return carry

    lax.fori_loop(0, n // 2, attend, 0)
    pass_on(5)
    lax.fori_loop(n // 2, n, attend, 0)
    attend_parts = []
    for h in range(heads):
        total = numer[h] / denom[h]
        gain = mixer_gain_ref[:, lanes(h, VHEAD_DIM)]
        attend_parts.append((total * normed(total, VHEAD_DIM) * gain).astype(bf16))
    attend_mixed = jnp.concatenate(attend_parts, axis=1)

    for k in (4, 5):
        local(k).wait()
        across(k, 0).wait_recv()
        on_line(k, False, lambda d: across(k, d).wait_recv())
    wc_ref, wa_ref = outs[3], outs[4]
    col_n = wc_ref.shape[2]
    part_rows = rows // heads_n
    for i in range(n):
        product = jnp.dot(chain_mixed, wc_ref[i], preferred_element_type=f32) + jnp.dot(
            attend_mixed, wa_ref[i], preferred_element_type=f32
        )
        for t in range(heads_n):
            send[t, :, lanes(i, col_n)] = product[lanes(t, part_rows)].astype(bf16)

    def sum_copy(d):
        return pltpu.make_async_remote_copy(
            src_ref=send.at[lax.rem(head + d, heads_n)],
            dst_ref=recv.at[d],
            send_sem=ss.at[d],
            recv_sem=rs.at[d],
            device_id=heads_peer(heads_n, d),
            device_id_type=MESH,
        )

    for d in range(1, heads_n):
        sum_copy(d).start()
    total = send[head].astype(f32)
    for d in range(1, heads_n):
        sum_copy(d).wait_recv()
        total = total + recv[d].astype(f32)
    out_ref[...] = total

    for d in range(1, heads_n):
        sum_copy(d).wait_send()
    for k in range(1 + count):
        across(k, 0).wait_send()
        on_line(k, True, lambda d: along(k, d).wait_send())
        on_line(k, False, lambda d: across(k, d).wait_send())
    for j in range(2):
        head_across(j, 0).wait_send()
        for d in range(1, head_lines):
            head_along(j, d).wait_send()
            head_across(j, d).wait_send()


def mix_all(n, heads_n, query, pair, blocks, others, heads):
    lines, head_lines = n // 2, heads_n // 2
    count = len(blocks)
    rows = query.shape[0]
    out_cols = n * blocks[-1].shape[1]
    vmem = pl.BlockSpec(memory_space=pltpu.VMEM)
    return pl.pallas_call(
        functools.partial(mixer_kernel, n, heads_n),
        out_shape=jax.ShapeDtypeStruct((rows // heads_n, out_cols), f32),
        in_specs=[vmem] * (2 + count + len(others)),
        out_specs=vmem,
        scratch_shapes=[
            pltpu.VMEM((heads_n,) + query.shape, query.dtype),
            pltpu.VMEM((heads_n, n) + pair.shape, pair.dtype),
        ]
        + [pltpu.VMEM((n,) + b.shape, b.dtype) for b in blocks]
        + [
            pltpu.VMEM((heads, rows, VHEAD_DIM), f32),
            pltpu.VMEM((heads, rows, 1), f32),
            pltpu.VMEM((heads_n, rows // heads_n, out_cols), bf16),
            pltpu.VMEM((heads_n, rows // heads_n, out_cols), bf16),
            pltpu.SemaphoreType.DMA((2 + count,)),
        ]
        + [pltpu.SemaphoreType.DMA((1 + count, lines))] * 4
        + [pltpu.SemaphoreType.DMA((2, head_lines))] * 4
        + [pltpu.SemaphoreType.DMA((heads_n,))] * 2,
        compiler_params=pltpu.CompilerParams(
            collective_id=1, has_side_effects=True, vmem_limit_bytes=VMEM_LIMIT
        ),
    )(query, pair, *blocks, *others)


def on_device(
    tokens,
    input_gain,
    chain_query,
    forward_gate,
    backward_gate,
    chain_value,
    output_gate,
    forget_rate,
    chain_gain,
    query_down,
    latent_down,
    rotary_down,
    query_latent_gain,
    latent_gain,
    query_up,
    latent_up,
    query_head_gain,
    key_head_gain,
    mixer_gain,
    chain_out,
    attend_out,
):
    n_sp, n_tp = lax.axis_size("sp"), lax.axis_size("tp")
    sp, tp = lax.axis_index("sp"), lax.axis_index("tp")
    rows, depth = tokens.shape[0], chain_query.shape[0]
    seq_len = rows * n_sp
    q_cols = query_down.shape[1] // n_tp
    l_cols = latent_down.shape[1] // n_tp
    r_cols = ROPE_DIM // n_tp
    q_down = lax.dynamic_slice_in_dim(query_down, tp * q_cols, q_cols, 1)
    l_down = jnp.concatenate(
        [
            lax.dynamic_slice_in_dim(latent_down, tp * l_cols, l_cols, 1),
            lax.dynamic_slice(rotary_down, (sp * depth, tp * r_cols), (depth, r_cols)),
        ],
        axis=1,
    )
    (v_rows, gate_logit, raw_q, raw_l, f_q, f_k, b_q, b_k, logs, f_state, b_state) = project_all(
        n_sp,
        tokens,
        input_gain[None],
        forget_rate,
        (chain_value, forward_gate, backward_gate, chain_query, output_gate, q_down, l_down),
    )

    heads = query_up.shape[1] // ATT_QK
    half = ROPE_DIM // 2
    inverse = rope_theta ** (-np.arange(0, ROPE_DIM, 2).astype(np.float32) / ROPE_DIM)
    angles = np.arange(seq_len, dtype=np.float32)[:, None] * inverse.astype(np.float32)
    cosine, sine = (
        jnp.asarray(np.tile(turn(angles), (1, 2)).reshape(n_sp, rows, ROPE_DIM), f32)
        for turn in (np.cos, np.sin)
    )

    def tails(gain):
        tail = gain[NOPE_DIM:]
        return jnp.stack([tail, jnp.roll(tail, half)])

    swap = np.zeros((ROPE_DIM, ROPE_DIM), np.float32)
    for j in range(half):
        swap[half + j, j] = -1.0
        swap[j, half + j] = 1.0
    pick_key = np.zeros((n_tp, l_cols + r_cols, ROPE_DIM), np.float32)
    for t in range(n_tp):
        for j in range(r_cols):
            pick_key[t, l_cols + j, t * r_cols + j] = 1.0
    pick_plain = np.zeros((heads, heads * ATT_QK, NOPE_DIM), np.float32)
    pick_query = np.zeros((heads, heads * ATT_QK, ROPE_DIM), np.float32)
    for h in range(heads):
        for j in range(NOPE_DIM):
            pick_plain[h, h * ATT_QK + j, j] = 1.0
        for j in range(ROPE_DIM):
            pick_query[h, h * ATT_QK + NOPE_DIM + j, j] = 1.0
    picks = [
        jnp.asarray(p, bf16)
        for p in (pick_key, pick_key @ swap, pick_plain, pick_query, pick_query @ swap)
    ]
    return mix_all(
        n_sp,
        n_tp,
        raw_q,
        raw_l,
        (logs, f_state, b_state, chain_out, attend_out),
        (
            f_q,
            f_k,
            b_q,
            b_k,
            v_rows,
            gate_logit,
            chain_gain[None],
            query_latent_gain.reshape(n_tp, 1, q_cols),
            latent_gain[None],
            query_up,
            latent_up,
            query_head_gain[None, :NOPE_DIM],
            key_head_gain[None, :NOPE_DIM],
            mixer_gain[None],
            tails(query_head_gain),
            tails(key_head_gain),
            cosine,
            sine,
            *picks,
        ),
        heads,
    )


def solution(mesh):
    placed = (
        P("sp", None),
        P(),
        P("sp", "tp"),
        P("sp", "tp"),
        P("sp", "tp"),
        P("sp", "tp"),
        P("sp", "tp"),
        P(None, "tp"),
        P("tp"),
        P("sp", None),
        P("sp", None),
        P(),
        P(),
        P(),
        P(None, "tp"),
        P(None, "tp"),
        P(),
        P(),
        P("tp"),
        P("tp", "sp"),
        P("tp", "sp"),
    )
    return jax.shard_map(
        on_device, mesh=mesh, in_specs=placed, out_specs=P(("sp", "tp"), None), check_vma=False
    )
```

profile of v0, /device:TPU:1, one launch (start us, length us, event | category | flops | bytes accessed | tf_op | source)
XLA Modules:
  0.0 135.1 jit_solution(6521789504058582405)
XLA Ops:
  0.0 0.0 copy-start
  0.0 0.0 copy-start.3
  0.0 0.0 copy-start.2
  0.0 0.7 copy-done.3
  0.7 0.0 copy-done.2
  0.7 0.6 slice_bitcast_fusion.2
  1.3 0.1 fusion.1
  1.4 0.1 maximum_bitcast_fusion
  1.5 0.6 pad_maximum_fusion.1.refs_21_
  2.1 0.1 fusion
  2.1 0.0 copy-start.1
  2.1 0.1 maximum_bitcast_fusion.1
  2.2 0.6 pad_maximum_fusion.2.refs_22_
  2.8 0.0 copy-done.1
  2.8 0.7 reshape.3.refs_14_
  3.5 0.0 dynamic-slice-start
  3.5 0.7 dynamic-slice-done
  4.2 0.1 copy.30
  4.3 0.8 constant_dynamic-slice_fusion
  5.2 0.7 pad_maximum_fusion.refs_9_
  5.8 0.0 copy-done
  5.8 0.8 constant_dynamic-slice_fusion.1.refs_8_
  6.6 61.5 %shard_map.262 = (bf16[160,256]{1,0:T(8,128)(2,1)}, bf16[160,256]{1,0:T(8,128)(2,1)}, bf16[160,192]{1,0:T(8,128)(2,1)}, bf16[160,144]{1,0:T(8,128)(2,1)}, bf16[1...) custom-call(bf16[160,2048]{1,0:T(8,128)(2,1)} %refs_0_.1, ...), custom_call_target="tpu_custom_call" | custom-call | tf_op jit(solution)/shard_map/pallas_call | solution.py:224
  68.1 65.3 %shard_map.263 = f32[40,2048]{1,0:T(8,128)} custom-call(bf16[160,192]{1,0:T(8,128)(2,1)} %get-tuple-element.16.refs_0_, bf16[160,144]{1,0:T(8,128)(2,1)} %get-tuple-element.17.refs_1_, f32[2,256]{1,0:T(2,128)} %get-tuple-element.18.refs_2_, bf16[128,256]{1,0:T(8,128)(2,1)} %get-tuple-element.19.refs_3_, bf16[128,256]{1,0:T(8,128)(2,1)} %get-tuple-element.20.refs_4_, ...), custom_call_target="tpu_custom_call" | custom-call | tf_op jit(solution)/shard_map/pallas_call | solution.py:598
  133.4 1.7 %copy.32 = f32[40,2048]{1,0:T(8,128)} copy(f32[40,2048]{1,0:T(8,128)} %shard_map.263) | data formatting | bytes 655360
Async XLA Ops:
  0.0 5.8 %copy-start = (bf16[256,768]{1,0:T(8,128)(2,1)S(1)}, bf16[256,768]{1,0:T(8,128)(2,1)}, u32[]{:S(2)}) copy-start(bf16[256,768]{1,0:T(8,128)(2,1)} %param.37) | copy-start | bytes 1179652
  0.0 0.7 copy-start.3
  0.0 0.7 copy-start.2
  2.1 0.7 copy-start.1
  3.5 0.7 dynamic-slice-start
where the time goes:
time: 135 us
  Pallas kernels  127 us (94%)
  local copies, waits for them, and re-layouts  6.31 us (5%)
  other arithmetic  1.99 us (1%)
    pallas_call x1, Pallas kernels, mix_all(): pl.pallas_call(functools.partial(mixer_kernel, n, heads_n), out_shape=jax...  65.3 us
    pallas_call x1, Pallas kernels, project_all(): pl.pallas_call(functools.partial(project_kernel, n, count), out_shape=[ja...  61.5 us

commit v1 on v0

v1 whole, which is shorter than its diff:
```python
import functools

import jax
import jax.numpy as jnp
import numpy as np
from jax import lax
from jax.experimental import pallas as pl
from jax.experimental.pallas import tpu as pltpu
from jax.sharding import PartitionSpec as P

LANES = 128
NOPE_DIM = 128
ROPE_DIM = 64
ATT_QK = 192
HALF = ROPE_DIM // 2

norm_eps = 1e-06
rope_theta = 10000.0
MESH = pl.DeviceIdType.MESH
VMEM_LIMIT = 60 * 1024 * 1024
f32 = jnp.float32
bf16 = jnp.bfloat16


def run_if(condition, act):
    if condition is None:
        act()
    else:
        pl.when(condition)(act)


def both(a, b):
    if a is None:
        return b
    if b is None:
        return a
    return jnp.logical_and(a, b)


def against(a, b):
    return lax.dot_general(a, b, (((1,), (1,)), ((), ())), preferred_element_type=f32)


def inverse_rms(values, size):
    return lax.rsqrt(jnp.sum(values * values, axis=-1, keepdims=True) / size + norm_eps)


def spread(count, start, signed):
    row = lax.broadcasted_iota(jnp.int32, (count, 3 * LANES), 0) - start
    col = lax.broadcasted_iota(jnp.int32, (count, 3 * LANES), 1)
    straight = (col < ATT_QK) & (row == col)
    at = col - 2 * LANES
    low = (at >= 0) & (at < HALF) & (row == NOPE_DIM + HALF + at)
    high = (at >= HALF) & (at < ROPE_DIM) & (row == NOPE_DIM + at - HALF)
    return (
        jnp.where(straight, 1.0, 0.0)
        + jnp.where(low, -1.0 if signed else 1.0, 0.0)
        + jnp.where(high, 1.0, 0.0)
    )


def mixer_kernel(n, heads_n, heads, sends, *refs):
    (
        tok_in,
        wv,
        wf,
        wb,
        wq,
        wg,
        q_down,
        l_down,
        rot_down,
        query_up,
        latent_up,
        chain_out,
        attend_out,
        rate_in,
        chain_gain_in,
        mixer_gain_in,
        input_gain,
        query_latent_gain,
        latent_gain,
        query_gain,
        key_gain,
        cos_row,
        sin_row,
        cos_block,
        sin_block,
        out_ref,
        stage,
        tok,
        xs,
        w_all,
        l_all,
        rot_all,
        lat,
        rate_ref,
        chain_gain_ref,
        mixer_gain_ref,
        up_q,
        up_l,
        kv,
        states,
        logs,
        mix_send,
        mix_recv,
        out_w,
        send,
        recv,
        ssem,
        r_tok,
        r_deliver,
        r_lat_w,
        r_rec_w,
        r_small,
        r_lat,
        r_kv,
        r_state,
        r_log,
        r_mix,
        r_out,
        r_sum,
    ) = refs
    mats = (wv, wf, wb, wq, wg)
    groups = ((0, 3), (3, 2))
    outer_n = 2 * heads
    inner_n = n // outer_n
    blocks = outer_n // 2
    part_rows, width = tok_in.shape[1:]
    rows = part_rows * heads_n
    q_units = q_down.shape[2] // LANES

    me = lax.axis_index("sp")
    t = lax.axis_index("tp")
    o, i = me // inner_n, lax.rem(me, inner_n)
    x, k = t // 2, lax.rem(t, 2)
    other = 1 - k
    at_home = (o // heads) == k
    away = jnp.logical_not(at_home)
    hh = lax.rem(o, heads)

    def dev(o_, i_, x_, k_):
        return {"sp": o_ * inner_n + i_, "tp": x_ * 2 + k_}

    def turn_o(d):
        return lax.rem(o + d, outer_n)

    def turn_i(d):
        return lax.rem(i + d, inner_n)

    def lane(index, size=LANES):
        return pl.ds(pl.multiple_of(index * size, LANES), size)

    peers = [dev(turn_o(d), i, x, r) for d in range(1, outer_n) for r in range(2)]
    peers += [dev(o, turn_i(d), x, k) for d in range(1, inner_n)]
    peers += [{"sp": me, "tp": lax.rem(t + d, heads_n)} for d in range(1, heads_n)]
    barrier = pltpu.get_barrier_semaphore()
    for peer in peers:
        pl.semaphore_signal(barrier, inc=1, device_id=peer, device_id_type=MESH)
    pl.semaphore_wait(barrier, len(peers))

    pending = []

    def copy(src, dst, send_sem, recv_sem, device):
        return pltpu.make_async_remote_copy(
            src_ref=src,
            dst_ref=dst,
            send_sem=send_sem,
            recv_sem=recv_sem,
            device_id=device,
            device_id_type=MESH,
        )

    def launch(src, dst, recv_sem, device, condition=None):
        index = len(pending)
        assert index < sends

        def make():
            return copy(src, dst, ssem.at[index], recv_sem, device)

        run_if(condition, lambda: make().start())
        pending.append((condition, lambda: make().wait_send()))

    def arrive(dst, recv_sem, condition=None):
        run_if(
            condition,
            lambda: copy(dst, dst, ssem.at[0], recv_sem, dev(o, i, x, other)).wait_recv(),
        )

    partner = dev(o, i, x, other)
    beside = dev(o, i, 1 - x, k)

    right, left = o + 1 < outer_n, o > 0
    launch(tok_in.at[t], stage.at[o], r_tok.at[o], dev(o + 1, i, x, k), right)
    launch(tok_in.at[t], stage.at[o], r_tok.at[o], dev(o - 1, i, x, k), left)

    is_q, is_l = x == 0, x != 0
    extra_o, extra_unit = 1 + x, outer_n + x
    extra = o == extra_o
    for d in range(1, outer_n):
        there = turn_o(d)
        for source, condition in ((q_down, is_q), (l_down, is_l)):
            launch(
                source.at[k, :, lane(there)],
                l_all.at[0, me, k],
                r_lat_w.at[0, me, k],
                dev(there, i, x, k),
                condition,
            )
    launch(
        q_down.at[k, :, lane(extra_unit)],
        l_all.at[1, me, k],
        r_lat_w.at[1, me, k],
        dev(extra_o, i, x, k),
        jnp.logical_not(extra),
    )

    def send_weights(g):
        first, count = groups[g]
        for m in range(first, first + count):
            for h in range(heads):
                there = heads * k + h
                for r in range(2):
                    launch(
                        mats[m].at[r, :, h * LANES : (h + 1) * LANES],
                        w_all.at[me, m, r],
                        r_rec_w.at[g, me, r],
                        dev(there, i, x, r),
                        jnp.logical_not((there == o) & (k == r)),
                    )

    for j, (source, target) in enumerate(
        (
            (query_up, up_q),
            (latent_up.at[:, lane(hh, 2 * LANES)], up_l),
            (rate_in, rate_ref),
            (chain_gain_in, chain_gain_ref),
            (mixer_gain_in, mixer_gain_ref),
        )
    ):
        launch(source, target, r_small.at[j], partner, at_home)
    send_weights(0)

    @pl.when(is_q)
    def _():
        l_all[0, me, k] = q_down[k, :, lane(o)]

    @pl.when(is_l)
    def _():
        l_all[0, me, k] = l_down[k, :, lane(o)]

    @pl.when(extra)
    def _():
        l_all[1, me, k] = q_down[k, :, lane(extra_unit)]

    @pl.when(at_home)
    def _():
        for m in range(len(mats)):
            w_all[me, m, k] = mats[m][k, :, lane(hh)]
        up_q[...] = query_up[...]
        up_l[...] = latent_up[:, lane(hh, 2 * LANES)]
        rate_ref[...] = rate_in[...]
        chain_gain_ref[...] = chain_gain_in[...]
        mixer_gain_ref[...] = mixer_gain_in[...]

    def lat_piece(slot, s, half):
        return l_all.at[slot, s, half], r_lat_w.at[slot, s, half]

    def rec_piece(g, s, half):
        first, count = groups[g]
        return w_all.at[s, first : first + count, half], r_rec_w.at[g, s, half]

    def pass_on(piece, s, condition=None):
        ref, sem = piece(s, k)
        for e in range(1, inner_n):
            launch(ref, ref, sem, dev(o, turn_i(e), x, k), condition)
        launch(ref, ref, sem, partner, condition)

    def from_lines(piece, first, condition=None, own=None):
        for d in range(first, outer_n):
            s = turn_o(d) * inner_n + i
            wait = condition if d else own
            if d or own is not None:
                arrive(*piece(s, k), wait)
            pass_on(piece, s, condition)

    def from_pairs(piece, condition=None):
        for e in range(1, inner_n):
            for d in range(outer_n):
                s = turn_o(d) * inner_n + turn_i(e)
                ref, sem = piece(s, k)
                arrive(ref, sem, condition)
                launch(ref, ref, sem, partner, condition)

    def from_partner(piece, condition=None):
        def wait_all():
            @pl.loop(0, n)
            def _(s):
                arrive(*piece(s, other))

        run_if(condition, wait_all)

    lat_a = functools.partial(lat_piece, 0)
    lat_b = functools.partial(lat_piece, 1)
    rec = [functools.partial(rec_piece, g) for g in range(2)]

    def own_line(piece, condition=None, own=None):
        if own is not None:
            arrive(*piece(me, k), own)
        pass_on(piece, me, condition)

    own_line(lat_a)
    own_line(lat_b, extra)

    for b in range(blocks):

        @pl.when(blocks * k + b == o)
        def _():
            tok[b] = tok_in[...]

    sign_pick = spread(ATT_QK, 0, True)[NOPE_DIM:, LANES:].astype(bf16)

    @pl.loop(0, n)
    def _(s):
        rot_all[s] = jnp.dot(rot_down[s], sign_pick, preferred_element_type=f32).astype(bf16)

    own_line(rec[0], None, away)

    def gains(ref):
        wide = jnp.broadcast_to(ref[...], (8, ATT_QK))
        return jnp.dot(
            wide,
            spread(ATT_QK, 0, False),
            precision=lax.Precision.HIGHEST,
            preferred_element_type=f32,
        )[0:1]

    for j, target in enumerate((up_q, up_l, rate_ref, chain_gain_ref, mixer_gain_ref)):
        arrive(target, r_small.at[j], away)
    up_q[...] = jnp.dot(
        up_q[...],
        spread(heads * ATT_QK, hh * ATT_QK, True).astype(bf16),
        preferred_element_type=f32,
    ).astype(bf16)

    def deliver(there, condition):
        core, b = there // blocks, lax.rem(there, blocks)
        launch(
            stage.at[there], tok.at[b, t], r_deliver.at[b, t], dev(o, i, 1 - x, core), condition
        )
        launch(
            stage.at[there],
            tok.at[b, t],
            r_deliver.at[b, t],
            partner,
            both(condition, core != k),
        )

        @pl.when(both(condition, core == k))
        def _():
            tok[b, t] = stage[there]

    for d in range(1, outer_n):
        for there, onward, step in ((o - d, right, 1), (o + d, left, -1)):
            valid = (there >= 0) & (there < outer_n)
            there = jnp.clip(there, 0, outer_n - 1)
            arrive(stage.at[there], r_tok.at[there], valid)
            launch(
                stage.at[there],
                stage.at[there],
                r_tok.at[there],
                dev(o + step, i, x, k),
                both(valid, onward),
            )
            deliver(there, valid)

    from_lines(lat_a, 1)
    from_lines(lat_b, 1, extra)
    from_pairs(lat_a)
    from_pairs(lat_b, extra)

    depth = width // n
    for b in range(blocks):
        there = blocks * k + b
        for d in range(1, heads_n):
            q = lax.rem(t + d, heads_n)
            arrive(tok.at[b, q], r_deliver.at[b, q], there != o)
        wide = jnp.concatenate([tok[b, q].astype(f32) for q in range(heads_n)], axis=0)
        scale = inverse_rms(wide, width)
        normed = (wide * scale * input_gain[...]).astype(bf16)
        for s in range(n):
            xs[s, b * rows : (b + 1) * rows, :] = normed[:, s * depth : (s + 1) * depth]

    def project(rhs, columns):
        def body(s, total):
            return total + jnp.dot(xs[s], rhs(s), preferred_element_type=f32)

        return lax.fori_loop(
            0, n, body, jnp.zeros((blocks * rows, columns), f32), unroll=n <= 8
        ).astype(bf16)

    from_partner(lat_a)
    from_partner(lat_b, extra)
    own_unit = x * q_units + o
    first = project(
        lambda s: jnp.concatenate([l_all[0, s].reshape(depth, LANES), rot_all[s]], axis=1),
        3 * LANES,
    )
    lat[own_unit] = first[:, :LANES]
    rotary = first[:, LANES:].astype(f32)

    @pl.when(extra)
    def _():
        lat[extra_unit] = project(lambda s: l_all[1, s].reshape(depth, LANES), LANES)

    def send_unit(unit, condition=None):
        for d in range(1, outer_n):
            launch(lat.at[unit], lat.at[unit], r_lat.at[unit], dev(turn_o(d), i, x, k), condition)
        launch(lat.at[unit], lat.at[unit], r_lat.at[unit], beside, condition)

    send_unit(own_unit)
    send_unit(extra_unit, extra)
    send_weights(1)

    def out_piece(j, s):
        return out_w.at[j, s], r_out.at[j, s]

    outs = (chain_out, attend_out)
    for j in range(2):
        for d in range(1, outer_n):
            ref, sem = out_piece(j, me)
            launch(outs[j], ref, sem, dev(turn_o(d), i, x, k))
        out_w[j, me] = outs[j][...]

    from_lines(rec[0], 1)

    def relay_unit(unit, condition=None):
        arrive(lat.at[unit], r_lat.at[unit], condition)
        launch(lat.at[unit], lat.at[unit], r_lat.at[unit], beside, condition)

    for d in range(1, outer_n):
        relay_unit(x * q_units + turn_o(d))
    relay_unit(extra_unit, jnp.logical_not(extra))
    from_pairs(rec[0])

    for d in range(outer_n):
        unit = (1 - x) * q_units + turn_o(d)
        arrive(lat.at[unit], r_lat.at[unit])
    far_unit = outer_n + 1 - x
    arrive(lat.at[far_unit], r_lat.at[far_unit])

    cosines, sines = [], []
    for b in range(blocks):
        s = (blocks * k + b) * inner_n + i
        cb, sb = cos_block[pl.ds(s, 1), :], sin_block[pl.ds(s, 1), :]
        cosines.append(cb * cos_row[...] - sb * sin_row[...])
        sines.append(sb * cos_row[...] + cb * sin_row[...])
    cosine = jnp.concatenate(cosines, axis=0)
    sine = jnp.concatenate(sines, axis=0)

    def latent(first_unit, count, gain):
        wide = jnp.concatenate(
            [lat[u].astype(f32) for u in range(first_unit, first_unit + count)], axis=1
        )
        return (wide * inverse_rms(wide, count * LANES) * gain[...]).astype(bf16)

    def finish(plain, tail, swapped, gain):
        square = jnp.sum(plain * plain + tail * tail, axis=-1, keepdims=True)
        scale = lax.rsqrt(square / ATT_QK + norm_eps)
        turned = tail * gain[:, LANES : 2 * LANES] * cosine + swapped * gain[:, 2 * LANES :] * sine
        return jnp.concatenate(
            [(plain * scale * gain[:, :LANES]).astype(bf16), (turned * scale).astype(bf16)], axis=1
        )

    pairs = jnp.dot(
        latent(q_units, outer_n, latent_gain), up_l[...], preferred_element_type=f32
    ).astype(bf16)
    kv[i, k, :, : 2 * LANES] = finish(
        pairs[:, :LANES].astype(f32), rotary[:, :LANES], rotary[:, LANES:], gains(key_gain)
    )
    kv[i, k, :, 2 * LANES :] = pairs[:, LANES:]

    def shared(ref, sem):
        for e in range(1, inner_n):
            launch(ref, ref, sem, dev(o, turn_i(e), x, k))
        launch(ref, ref, sem, partner)

    shared(kv.at[i, k], r_kv.at[i, k])

    attend_q = (
        jnp.dot(latent(0, q_units, query_latent_gain), up_q[...], preferred_element_type=f32)
        .astype(bf16)
        .astype(f32)
    )
    query = finish(
        attend_q[:, :LANES],
        attend_q[:, LANES : 2 * LANES],
        attend_q[:, 2 * LANES :],
        gains(query_gain),
    )

    def columns(s, mats_here):
        return jnp.concatenate([w_all[s, m].reshape(depth, LANES) for m in mats_here], axis=1)

    from_partner(rec[0])
    vfb = project(lambda s: columns(s, (0, 1, 2)), 3 * LANES)
    value = [vfb[b * rows : (b + 1) * rows, :LANES] for b in range(blocks)]
    row = lax.broadcasted_iota(jnp.int32, (rows, rows), 0)
    col = lax.broadcasted_iota(jnp.int32, (rows, rows), 1)
    masks = (row >= col, row <= col)

    def direction(d):
        rate = rate_ref[d : d + 1, lane(hh)] / (rows * n)
        logit = vfb[:, (1 + d) * LANES : (2 + d) * LANES].astype(f32)
        key = rate * jax.nn.sigmoid(-logit)
        decay = jnp.log1p(-key)
        total = jnp.dot(
            jnp.where(masks[d], 1.0, 0.0),
            jnp.concatenate([decay[b * rows : (b + 1) * rows] for b in range(blocks)], axis=1),
            precision=lax.Precision.HIGHEST,
            preferred_element_type=f32,
        )
        keys, totals = [], []
        last = (rows - 1, 0)[d]
        for b in range(blocks):
            part = total[:, b * LANES : (b + 1) * LANES]
            full = part[last : last + 1, :]
            near = (key[b * rows : (b + 1) * rows] * jnp.exp(-part)).astype(bf16)
            state = lax.dot_general(
                value[b], near, (((0,), (0,)), ((), ())), preferred_element_type=f32
            )
            states[i, blocks * k + b, d] = (state * jnp.exp(full)).astype(bf16)
            logs[i, blocks * k + b, d] = jnp.broadcast_to(full, (8, LANES))
            keys.append(near)
            totals.append(part)
        return keys, totals

    near = [direction(d) for d in range(2)]

    def state_pieces(i_, k_):
        at = pl.ds(k_ * blocks, blocks)
        return (states.at[i_, at], r_state.at[i_, k_]), (logs.at[i_, at], r_log.at[i_, k_])

    for ref, sem in state_pieces(i, k):
        shared(ref, sem)

    own_line(rec[1], None, away)
    from_lines(rec[1], 1)
    for j in range(2):
        ref, sem = out_piece(j, me)
        for e in range(1, inner_n):
            launch(outs[j], ref, sem, dev(o, turn_i(e), x, k))

    scale = ATT_QK ** (-0.5) * 1.4426950408889634

    def attend(carry, i_, k_):
        numer, denom = carry
        score = against(query, kv[i_, k_, :, : 2 * LANES])
        weight = jnp.exp2(score * scale)
        numer += jnp.dot(
            weight.astype(bf16), kv[i_, k_, :, 2 * LANES :], preferred_element_type=f32
        )
        return numer, denom + jnp.sum(weight, axis=-1, keepdims=True)

    carry = (jnp.zeros((blocks * rows, LANES), f32), jnp.zeros((blocks * rows, 1), f32))
    carry = attend(carry, i, k)
    arrive(kv.at[i, other], r_kv.at[i, other])
    carry = attend(carry, i, other)

    def relay_pair(ref, sem):
        arrive(ref, sem)
        launch(ref, ref, sem, partner)

    for e in range(1, inner_n):
        relay_pair(kv.at[turn_i(e), k], r_kv.at[turn_i(e), k])
    for e in range(1, inner_n):
        for ref, sem in state_pieces(turn_i(e), k):
            relay_pair(ref, sem)
    from_pairs(rec[1])
    for e in range(1, inner_n):
        there = turn_i(e)
        carry = attend(carry, there, k)
        arrive(kv.at[there, other], r_kv.at[there, other])
        carry = attend(carry, there, other)
    rows_out = carry[0] / carry[1]
    attend_mixed = (
        rows_out * inverse_rms(rows_out, LANES) * mixer_gain_ref[:, lane(hh)]
    ).astype(bf16)

    for j in range(2):
        for d in range(1, outer_n):
            s = turn_o(d) * inner_n + i
            ref, sem = out_piece(j, s)
            arrive(ref, sem)
            for e in range(1, inner_n):
                launch(ref, ref, sem, dev(o, turn_i(e), x, k))

    from_partner(rec[1])
    qg = project(lambda s: columns(s, (3, 4)), 2 * LANES).astype(f32)
    for e in range(inner_n):
        for k_ in (k, other):
            if e or k_ is other:
                for ref, sem in state_pieces(turn_i(e), k_):
                    if k_ is other:
                        arrive(ref, sem)

    def forward(s, state):
        i_, o_ = lax.rem(s, inner_n), s // inner_n
        return state * jnp.exp(logs[i_, o_, 0, 0:1, :]) + states[i_, o_, 0].astype(f32)

    def backward(j, state):
        s = n - 1 - j
        i_, o_ = lax.rem(s, inner_n), s // inner_n
        return state * jnp.exp(logs[i_, o_, 1, 0:1, :]) + states[i_, o_, 1].astype(f32)

    nothing = jnp.zeros((LANES, LANES), f32)
    for b in range(blocks):
        there = blocks * k + b
        s = there * inner_n + i
        incoming = (
            lax.fori_loop(0, s, forward, nothing).astype(bf16),
            lax.fori_loop(0, n - 1 - s, backward, nothing).astype(bf16),
        )
        at = slice(b * rows, (b + 1) * rows)
        total = jnp.zeros((rows, LANES), f32)
        within = jnp.zeros((rows, rows), f32)
        for d in range(2):
            keys, totals = near[d]
            probe = (qg[at, :LANES] * jnp.exp(totals[b])).astype(bf16)
            within += jnp.where(masks[d], against(probe, keys[b]), 0.0)
            total += against(probe, incoming[d])
        total += jnp.dot(within.astype(bf16), value[b], preferred_element_type=f32)
        gate = qg[at, LANES:]
        scaled = total * inverse_rms(total, LANES) * chain_gain_ref[:, lane(hh)]
        mix_send[b, :, :LANES] = (scaled * (gate * jax.nn.sigmoid(gate))).astype(bf16)
        mix_send[b, :, LANES:] = attend_mixed[at]
        home = there == o
        launch(
            mix_send.at[b],
            mix_recv.at[hh],
            r_mix.at[hh],
            dev(there, i, x, o // heads),
            jnp.logical_not(home),
        )

        @pl.when(home)
        def _():
            mix_recv[hh] = mix_send[b]

    for j in range(2):
        for e in range(1, inner_n):
            for d in range(outer_n):
                arrive(*out_piece(j, turn_o(d) * inner_n + turn_i(e)))
    for h in range(heads):
        arrive(mix_recv.at[h], r_mix.at[h], heads * k + h != o)
    chain_mixed = jnp.concatenate([mix_recv[h, :, :LANES] for h in range(heads)], axis=1)
    attended = jnp.concatenate([mix_recv[h, :, LANES:] for h in range(heads)], axis=1)
    col_n = out_w.shape[3]
    for s in range(n):
        product = jnp.dot(chain_mixed, out_w[0, s], preferred_element_type=f32) + jnp.dot(
            attended, out_w[1, s], preferred_element_type=f32
        )
        for q in range(heads_n):
            send[q, :, s * col_n : (s + 1) * col_n] = product[
                q * part_rows : (q + 1) * part_rows
            ].astype(bf16)
    for d in range(1, heads_n):
        there = lax.rem(t + d, heads_n)
        launch(send.at[there], recv.at[d], r_sum.at[d], {"sp": me, "tp": there})
    total = send[t].astype(f32)
    for d in range(1, heads_n):
        arrive(recv.at[d], r_sum.at[d])
        total = total + recv[d].astype(f32)
    out_ref[...] = total
    for condition, finish_send in pending:
        run_if(condition, finish_send)


def on_device(
    tokens,
    input_gain,
    chain_query,
    forward_gate,
    backward_gate,
    chain_value,
    output_gate,
    forget_rate,
    chain_gain,
    query_down,
    latent_down,
    rotary_down,
    query_latent_gain,
    latent_gain,
    query_up,
    latent_up,
    query_head_gain,
    key_head_gain,
    mixer_gain,
    chain_out,
    attend_out,
):
    n, heads_n = lax.axis_size("sp"), lax.axis_size("tp")
    rows, width = tokens.shape
    depth = chain_query.shape[0]
    heads = query_up.shape[1] // ATT_QK
    outer_n = 2 * heads
    inner_n = n // outer_n
    blocks = outer_n // 2
    half = depth // 2
    units = (query_down.shape[1] + latent_down.shape[1]) // LANES
    part = rows // heads_n
    out_cols = n * chain_out.shape[1]

    inverse = rope_theta ** (-np.arange(0, ROPE_DIM, 2) / ROPE_DIM)

    def table(positions):
        angles = np.tile(positions[:, None] * inverse, (1, 2))
        pad = ((0, 0), (0, LANES - ROPE_DIM))
        return [jnp.asarray(np.pad(f(angles), pad), f32) for f in (np.cos, np.sin)]

    in_row = table(np.arange(rows, dtype=np.float64))
    in_block = table(np.arange(n, dtype=np.float64) * rows)

    def halves(w):
        return w.reshape(2, half, w.shape[1])

    operands = (
        tokens.reshape(heads_n, part, width),
        *[
            halves(w)
            for w in (
                chain_value,
                forward_gate,
                backward_gate,
                chain_query,
                output_gate,
                query_down,
                latent_down,
            )
        ],
        rotary_down.reshape(n, depth, ROPE_DIM),
        query_up,
        latent_up,
        chain_out,
        attend_out,
        forget_rate,
        chain_gain[None],
        mixer_gain[None],
        input_gain[None],
        query_latent_gain[None],
        latent_gain[None],
        query_head_gain[None],
        key_head_gain[None],
        *in_row,
        *in_block,
    )
    sends = 120 + 26 * n
    dma = pltpu.SemaphoreType.DMA
    vmem = pl.BlockSpec(memory_space=pltpu.VMEM)
    tall = blocks * rows
    return pl.pallas_call(
        functools.partial(mixer_kernel, n, heads_n, heads, sends),
        out_shape=jax.ShapeDtypeStruct((part, out_cols), f32),
        in_specs=[vmem] * len(operands),
        out_specs=vmem,
        scratch_shapes=[
            pltpu.VMEM((outer_n, part, width), bf16),
            pltpu.VMEM((blocks, heads_n, part, width), bf16),
            pltpu.VMEM((n, tall, depth), bf16),
            pltpu.VMEM((n, 5, 2, half, LANES), bf16),
            pltpu.VMEM((2, n, 2, half, LANES), bf16),
            pltpu.VMEM((n, depth, 2 * LANES), bf16),
            pltpu.VMEM((units, tall, LANES), bf16),
            pltpu.VMEM(forget_rate.shape, f32),
            pltpu.VMEM((1,) + chain_gain.shape, f32),
            pltpu.VMEM((1,) + mixer_gain.shape, f32),
            pltpu.VMEM(query_up.shape, bf16),
            pltpu.VMEM((latent_up.shape[0], 2 * LANES), bf16),
            pltpu.VMEM((inner_n, 2, tall, 3 * LANES), bf16),
            pltpu.VMEM((inner_n, outer_n, 2, LANES, LANES), bf16),
            pltpu.VMEM((inner_n, outer_n, 2, 8, LANES), f32),
            pltpu.VMEM((blocks, rows, 2 * LANES), bf16),
            pltpu.VMEM((heads, rows, 2 * LANES), bf16),
            pltpu.VMEM((2, n) + chain_out.shape, bf16),
            pltpu.VMEM((heads_n, part, out_cols), bf16),
            pltpu.VMEM((heads_n, part, out_cols), bf16),
            dma((sends,)),
            dma((outer_n,)),
            dma((blocks, heads_n)),
            dma((2, n, 2)),
            dma((2, n, 2)),
            dma((5,)),
            dma((units,)),
            dma((inner_n, 2)),
            dma((inner_n, 2)),
            dma((inner_n, 2)),
            dma((heads,)),
            dma((2, n)),
            dma((heads_n,)),
        ],
        compiler_params=pltpu.CompilerParams(
            collective_id=0, has_side_effects=True, vmem_limit_bytes=VMEM_LIMIT
        ),
    )(*operands)


def solution(mesh):
    placed = (
        P("sp", None),
        P(),
        P("sp", "tp"),
        P("sp", "tp"),
        P("sp", "tp"),
        P("sp", "tp"),
        P("sp", "tp"),
        P(None, "tp"),
        P("tp"),
        P("sp", None),
        P("sp", None),
        P(),
        P(),
        P(),
        P(None, "tp"),
        P(None, "tp"),
        P(),
        P(),
        P("tp"),
        P("tp", "sp"),
        P("tp", "sp"),
    )
    return jax.shard_map(
        on_device, mesh=mesh, in_specs=placed, out_specs=P(("sp", "tp"), None), check_vma=False
    )
```

time: 135 us -> 114 us (0.84)
  the two profiles are of different devices: /device:TPU:1 before, /device:TPU:13 now
where the time goes in v1:
time: 114 us
  Pallas kernels  109 us (96%)
  local copies, waits for them, and re-layouts  4.93 us (4%)
    pallas_call x1, Pallas kernels, on_device(): pl.pallas_call(functools.partial(mixer_kernel, n, heads_n, heads, sends),...  109 us
    unnamed x4, local copies, waits for them, and re-layouts  4.35 us

profile of v1, /device:TPU:13, one launch (start us, length us, event | category | flops | bytes accessed | tf_op | source)
XLA Modules:
  0.0 114.1 jit_solution(15271125271976737172)
XLA Ops:
  0.0 0.0 copy-start
  0.0 0.7 copy-done
  0.7 0.6 broadcast_in_dim.24.refs_17_
  1.3 1.9 %copy.26 = bf16[2048,64]{1,0:T(8,128)(2,1)} copy(bf16[2048,64]{0,1:T(8,128)(2,1)} %param.36) | data formatting | bytes 524288 | tf_op args[11]
  3.2 109.1 %shard_map.235 = f32[40,2048]{1,0:T(8,128)} custom-call(bf16[4,40,2048]{2,1,0:T(8,128)(2,1)} %bitcast.16, bf16[2,128,256]{2,1,0:T(8,128)(2,1)} %bitcast.19, bf16[2,128,256]{2,1,0:T(8,128)(2,1)} %bitcast.20, bf16[2,128,256]{2,1,0:T(8,128)(2,1)} %bitcast.21, bf16[2,128,256]{2,1,0:T(8,128)(2,1)} %bitcast.22, bf16[2,128,256]{2,1,0:T(8,128)(2,1)} %bitcast.23, ...), custom_call_target="tpu_custom_call" | custom-call | tf_op jit(solution)/shard_map/pallas_call | solution.py:761
  112.3 1.7 %copy.28 = f32[40,2048]{1,0:T(8,128)} copy(f32[40,2048]{1,0:T(8,128)} %shard_map.235) | data formatting | bytes 655360
Async XLA Ops:
  0.0 0.7 copy-start

commit v2 on v1

--- a/solution.py
+++ b/solution.py
@@ -59,7 +59,10 @@
     )
 
 
-def mixer_kernel(n, heads_n, heads, sends, *refs):
+def mixer_kernel(n, heads_n, heads, sends, needed, *refs):
+    count = 13
+    far, near_by = refs[:count], refs[-count - 1 : -1]
+    fetched = refs[-1]
     (
         tok_in,
         wv,
@@ -74,6 +77,8 @@
         latent_up,
         chain_out,
         attend_out,
+    ) = near_by
+    (
         rate_in,
         chain_gain_in,
         mixer_gain_in,
@@ -105,13 +110,21 @@
         mix_send,
         mix_recv,
         out_w,
-        send,
-        recv,
+        part_far,
+        part_near,
+        send_far,
+        send_near,
+        got_far,
+        got_near,
+        send_x,
+        got_x,
         ssem,
         r_tok,
         r_deliver,
         r_lat_w,
+        r_lat_p,
         r_rec_w,
+        r_rec_p,
         r_small,
         r_lat,
         r_kv,
@@ -120,13 +133,14 @@
         r_mix,
         r_out,
         r_sum,
-    ) = refs
+    ) = refs[count : -count - 1]
     mats = (wv, wf, wb, wq, wg)
     groups = ((0, 3), (3, 2))
     outer_n = 2 * heads
     inner_n = n // outer_n
     blocks = outer_n // 2
     part_rows, width = tok_in.shape[1:]
+    chunk = width // 2
     rows = part_rows * heads_n
     q_units = q_down.shape[2] // LANES
 
@@ -154,12 +168,15 @@
     peers = [dev(turn_o(d), i, x, r) for d in range(1, outer_n) for r in range(2)]
     peers += [dev(o, turn_i(d), x, k) for d in range(1, inner_n)]
     peers += [{"sp": me, "tp": lax.rem(t + d, heads_n)} for d in range(1, heads_n)]
+    fetches = [pltpu.make_async_copy(far[j], near_by[j], fetched.at[j]) for j in range(count)]
+    for fetch in fetches:
+        fetch.start()
     barrier = pltpu.get_barrier_semaphore()
     for peer in peers:
         pl.semaphore_signal(barrier, inc=1, device_id=peer, device_id_type=MESH)
     pl.semaphore_wait(barrier, len(peers))
 
-    pending = []
+    pending, spare, used = [], [], [0]
 
     def copy(src, dst, send_sem, recv_sem, device):
         return pltpu.make_async_remote_copy(
@@ -171,15 +188,37 @@
             device_id_type=MESH,
         )
 
-    def launch(src, dst, recv_sem, device, condition=None):
-        index = len(pending)
-        assert index < sends
+    def launch(src, dst, recv_sem, device, condition=None, index=None):
+        if index is None:
+            if not spare:
+                spare.append(used[0])
+                used[0] += 1
+            index = spare.pop(0)
+        assert used[0] <= sends
 
         def make():
             return copy(src, dst, ssem.at[index], recv_sem, device)
 
         run_if(condition, lambda: make().start())
-        pending.append((condition, lambda: make().wait_send()))
+        pending.append((condition, lambda: make().wait_send(), index))
+        return index
+
+    def reserve(size):
+        base = used[0]
+        used[0] += size
+        return base
+
+    def by_distance(d, act):
+        for there, toward in ((o - d, 1), (o + d, -1)):
+            valid = (there >= 0) & (there < outer_n)
+            act(jnp.clip(there, 0, outer_n - 1), valid, toward)
+
+    def drain(first):
+        for condition, finish_send, index in pending[:first]:
+            run_if(condition, finish_send)
+            if isinstance(index, int) and index not in spare:
+                spare.append(index)
+        del pending[:first]
 
     def arrive(dst, recv_sem, condition=None):
         run_if(
@@ -191,29 +230,43 @@
     beside = dev(o, i, 1 - x, k)
 
     right, left = o + 1 < outer_n, o > 0
-    launch(tok_in.at[t], stage.at[o], r_tok.at[o], dev(o + 1, i, x, k), right)
-    launch(tok_in.at[t], stage.at[o], r_tok.at[o], dev(o - 1, i, x, k), left)
+    halves = [slice(c * chunk, (c + 1) * chunk) for c in range(2)]
+    fetches[0].wait()
+    for c, at in enumerate(halves):
+        for step, condition in ((1, right), (-1, left)):
+            launch(
+                tok_in.at[t, :, at],
+                stage.at[c, o],
+                r_tok.at[c, o],
+                dev(o + step, i, x, k),
+                condition,
+            )
 
     is_q, is_l = x == 0, x != 0
     extra_o, extra_unit = 1 + x, outer_n + x
     extra = o == extra_o
+    for fetch in fetches[6:8]:
+        fetch.wait()
     for d in range(1, outer_n):
-        there = turn_o(d)
+        there, index = turn_o(d), None
         for source, condition in ((q_down, is_q), (l_down, is_l)):
-            launch(
+            index = launch(
                 source.at[k, :, lane(there)],
-                l_all.at[0, me, k],
-                r_lat_w.at[0, me, k],
+                l_all.at[0, i, o, k],
+                r_lat_w.at[0, i, o],
                 dev(there, i, x, k),
                 condition,
+                index,
             )
     launch(
         q_down.at[k, :, lane(extra_unit)],
-        l_all.at[1, me, k],
-        r_lat_w.at[1, me, k],
+        l_all.at[1, i, o, k],
+        r_lat_w.at[1, i, o],
         dev(extra_o, i, x, k),
         jnp.logical_not(extra),
     )
+    for fetch in fetches[1:6] + fetches[8:]:
+        fetch.wait()
 
     def send_weights(g):
         first, count = groups[g]
@@ -223,12 +276,28 @@
                 for r in range(2):
                     launch(
                         mats[m].at[r, :, h * LANES : (h + 1) * LANES],
-                        w_all.at[me, m, r],
-                        r_rec_w.at[g, me, r],
+                        w_all.at[i, o, m, r],
+                        r_rec_w.at[g, i, o],
                         dev(there, i, x, r),
-                        jnp.logical_not((there == o) & (k == r)),
+                        there != o,
                     )
 
+    def send_home_weights(g):
+        first, count = groups[g]
+        for m in range(first, first + count):
+            launch(
+                mats[m].at[other, :, lane(hh)],
+                w_all.at[i, o, m, other],
+                r_rec_w.at[g, i, o],
+                partner,
+                at_home,
+            )
+
+    def out_piece(j, i_, o_):
+        return out_w.at[j, i_, o_], r_out.at[j, i_, o_]
+
+    outs = (chain_out, attend_out)
+    send_home_weights(0)
     for j, (source, target) in enumerate(
         (
             (query_up, up_q),
@@ -239,76 +308,83 @@
         )
     ):
         launch(source, target, r_small.at[j], partner, at_home)
-    send_weights(0)
+    send_home_weights(1)
 
     @pl.when(is_q)
     def _():
-        l_all[0, me, k] = q_down[k, :, lane(o)]
+        l_all[0, i, o, k] = q_down[k, :, lane(o)]
 
     @pl.when(is_l)
     def _():
-        l_all[0, me, k] = l_down[k, :, lane(o)]
+        l_all[0, i, o, k] = l_down[k, :, lane(o)]
 
     @pl.when(extra)
     def _():
-        l_all[1, me, k] = q_down[k, :, lane(extra_unit)]
+        l_all[1, i, o, k] = q_down[k, :, lane(extra_unit)]
 
     @pl.when(at_home)
     def _():
         for m in range(len(mats)):
-            w_all[me, m, k] = mats[m][k, :, lane(hh)]
+            w_all[i, o, m, k] = mats[m][k, :, lane(hh)]
         up_q[...] = query_up[...]
         up_l[...] = latent_up[:, lane(hh, 2 * LANES)]
         rate_ref[...] = rate_in[...]
         chain_gain_ref[...] = chain_gain_in[...]
         mixer_gain_ref[...] = mixer_gain_in[...]
 
-    def lat_piece(slot, s, half):
-        return l_all.at[slot, s, half], r_lat_w.at[slot, s, half]
-
-    def rec_piece(g, s, half):
+    def lat_piece(slot, i_, o_):
+        return l_all.at[slot, i_, o_, k], r_lat_w.at[slot, i_, o_]
+
+    def lat_block(slot, i_, half):
+        return l_all.at[slot, i_, :, half], r_lat_p.at[slot, i_]
+
+    def rec_piece(g, i_, o_):
         first, count = groups[g]
-        return w_all.at[s, first : first + count, half], r_rec_w.at[g, s, half]
-
-    def pass_on(piece, s, condition=None):
-        ref, sem = piece(s, k)
+        return w_all.at[i_, o_, first : first + count, k], r_rec_w.at[g, i_, o_]
+
+    def rec_block(g, i_, half):
+        first, count = groups[g]
+        return w_all.at[i_, :, first : first + count, half], r_rec_p.at[g, i_]
+
+    def own_line(piece, condition=None, own=None):
+        ref, sem = piece[0](i, o)
+        if own is not None:
+            arrive(ref, sem, own)
         for e in range(1, inner_n):
             launch(ref, ref, sem, dev(o, turn_i(e), x, k), condition)
-        launch(ref, ref, sem, partner, condition)
-
-    def from_lines(piece, first, condition=None, own=None):
-        for d in range(first, outer_n):
-            s = turn_o(d) * inner_n + i
-            wait = condition if d else own
-            if d or own is not None:
-                arrive(*piece(s, k), wait)
-            pass_on(piece, s, condition)
+
+    def from_line(piece, d, condition=None):
+        def act(there, valid, toward):
+            valid = both(valid, condition)
+            ref, sem = piece[0](i, there)
+            arrive(ref, sem, valid)
+            for e in range(1, inner_n):
+                launch(ref, ref, sem, dev(o, turn_i(e), x, k), valid, piece[2][e] + there)
+
+        by_distance(d, act)
+        if d == outer_n - 1:
+            launch(*pair(piece[1], i, k), partner, condition)
+
+    def pair(block, i_, half):
+        ref, sem = block(i_, half)
+        return ref, ref, sem
 
     def from_pairs(piece, condition=None):
         for e in range(1, inner_n):
             for d in range(outer_n):
-                s = turn_o(d) * inner_n + turn_i(e)
-                ref, sem = piece(s, k)
-                arrive(ref, sem, condition)
-                launch(ref, ref, sem, partner, condition)
+                arrive(*piece[0](turn_i(e), turn_o(d)), condition)
+            launch(*pair(piece[1], turn_i(e), k), partner, condition)
 
     def from_partner(piece, condition=None):
-        def wait_all():
-            @pl.loop(0, n)
-            def _(s):
-                arrive(*piece(s, other))
-
-        run_if(condition, wait_all)
-
-    lat_a = functools.partial(lat_piece, 0)
-    lat_b = functools.partial(lat_piece, 1)
-    rec = [functools.partial(rec_piece, g) for g in range(2)]
-
-    def own_line(piece, condition=None, own=None):
-        if own is not None:
-            arrive(*piece(me, k), own)
-        pass_on(piece, me, condition)
-
+        for e in range(inner_n):
+            arrive(*piece[1](turn_i(e), other), condition)
+
+    def kind(piece, block, which):
+        marks = [reserve(outer_n) for _ in range(inner_n)]
+        return functools.partial(piece, which), functools.partial(block, which), marks
+
+    lat_a, lat_b = kind(lat_piece, lat_block, 0), kind(lat_piece, lat_block, 1)
+    rec = [kind(rec_piece, rec_block, g) for g in range(2)]
     own_line(lat_a)
     own_line(lat_b, extra)
 
@@ -319,12 +395,20 @@
             tok[b] = tok_in[...]
 
     sign_pick = spread(ATT_QK, 0, True)[NOPE_DIM:, LANES:].astype(bf16)
-
-    @pl.loop(0, n)
-    def _(s):
-        rot_all[s] = jnp.dot(rot_down[s], sign_pick, preferred_element_type=f32).astype(bf16)
+    depth = width // n
+    rot_all[...] = (
+        lax.dot_general(
+            rot_down[...], sign_pick, (((0,), (0,)), ((), ())), preferred_element_type=f32
+        )
+        .astype(bf16)
+        .reshape(n, depth, 2 * LANES)
+    )
 
     own_line(rec[0], None, away)
+    for j in range(2):
+        for e in range(1, inner_n):
+            launch(outs[j], *out_piece(j, i, o), dev(o, turn_i(e), x, k))
+    own_line(rec[1], None, away)
 
     def gains(ref):
         wide = jnp.broadcast_to(ref[...], (8, ATT_QK))
@@ -343,48 +427,53 @@
         preferred_element_type=f32,
     ).astype(bf16)
 
-    def deliver(there, condition):
+    marks = [[reserve(outer_n) for _ in range(3)] for _ in range(2)]
+
+    def relay_tokens(c, there, valid, toward, last):
+        ref, sem = stage.at[c, there], r_tok.at[c, there]
+        arrive(ref, sem, valid)
+        if not last:
+            onward = both(valid, right if toward > 0 else left)
+            launch(ref, ref, sem, dev(o + toward, i, x, k), onward, marks[c][0] + there)
         core, b = there // blocks, lax.rem(there, blocks)
-        launch(
-            stage.at[there], tok.at[b, t], r_deliver.at[b, t], dev(o, i, 1 - x, core), condition
-        )
-        launch(
-            stage.at[there],
-            tok.at[b, t],
-            r_deliver.at[b, t],
-            partner,
-            both(condition, core != k),
-        )
-
-        @pl.when(both(condition, core == k))
+        at = halves[c]
+        target, sem = tok.at[b, t, :, at], r_deliver.at[c, b, t]
+        launch(ref, target, sem, dev(o, i, 1 - x, core), valid, marks[c][1] + there)
+        launch(ref, target, sem, partner, both(valid, core != k), marks[c][2] + there)
+
+        @pl.when(both(valid, core == k))
         def _():
-            tok[b, t] = stage[there]
+            tok[b, t, :, at] = stage[c, there]
 
     for d in range(1, outer_n):
-        for there, onward, step in ((o - d, right, 1), (o + d, left, -1)):
-            valid = (there >= 0) & (there < outer_n)
-            there = jnp.clip(there, 0, outer_n - 1)
-            arrive(stage.at[there], r_tok.at[there], valid)
-            launch(
-                stage.at[there],
-                stage.at[there],
-                r_tok.at[there],
-                dev(o + step, i, x, k),
-                both(valid, onward),
+        for c in range(2):
+            by_distance(
+                d,
+                functools.partial(
+                    lambda c, there, valid, toward: relay_tokens(
+                        c, there, valid, toward, d == outer_n - 1
+                    ),
+                    c,
+                ),
             )
-            deliver(there, valid)
-
-    from_lines(lat_a, 1)
-    from_lines(lat_b, 1, extra)
+        if d == 1:
+            from_line(lat_a, 1)
+            from_line(lat_b, 1, extra)
+        if d == outer_n - 2:
+            send_weights(0)
+            for far_d in range(2, outer_n):
+                from_line(lat_a, far_d)
+                from_line(lat_b, far_d, extra)
+
     from_pairs(lat_a)
     from_pairs(lat_b, extra)
 
-    depth = width // n
     for b in range(blocks):
         there = blocks * k + b
         for d in range(1, heads_n):
             q = lax.rem(t + d, heads_n)
-            arrive(tok.at[b, q], r_deliver.at[b, q], there != o)
+            for c, at in enumerate(halves):
+                arrive(tok.at[b, q, :, at], r_deliver.at[c, b, q], there != o)
         wide = jnp.concatenate([tok[b, q].astype(f32) for q in range(heads_n)], axis=0)
         scale = inverse_rms(wide, width)
         normed = (wide * scale * input_gain[...]).astype(bf16)
@@ -403,7 +492,7 @@
     from_partner(lat_b, extra)
     own_unit = x * q_units + o
     first = project(
-        lambda s: jnp.concatenate([l_all[0, s].reshape(depth, LANES), rot_all[s]], axis=1),
+        lambda s: jnp.concatenate([l_all[0, lax.rem(s, inner_n), s // inner_n].reshape(depth, LANES), rot_all[s]], axis=1),
         3 * LANES,
     )
     lat[own_unit] = first[:, :LANES]
@@ -411,96 +500,73 @@
 
     @pl.when(extra)
     def _():
-        lat[extra_unit] = project(lambda s: l_all[1, s].reshape(depth, LANES), LANES)
+        lat[extra_unit] = project(lambda s: l_all[1, lax.rem(s, inner_n), s // inner_n].reshape(depth, LANES), LANES)
 
     def send_unit(unit, condition=None):
         for d in range(1, outer_n):
             launch(lat.at[unit], lat.at[unit], r_lat.at[unit], dev(turn_o(d), i, x, k), condition)
         launch(lat.at[unit], lat.at[unit], r_lat.at[unit], beside, condition)
 
+    early = len(pending)
     send_unit(own_unit)
     send_unit(extra_unit, extra)
+    for d in range(1, outer_n):
+        from_line(rec[0], d)
+
+    marks_x = reserve(outer_n)
+
+    def relay_unit(there, valid, toward):
+        unit = x * q_units + there
+        arrive(lat.at[unit], r_lat.at[unit], valid)
+        launch(lat.at[unit], lat.at[unit], r_lat.at[unit], beside, valid, marks_x + there)
+
+    for d in range(1, outer_n):
+        by_distance(d, relay_unit)
+    arrive(lat.at[extra_unit], r_lat.at[extra_unit], jnp.logical_not(extra))
+    launch(
+        lat.at[extra_unit],
+        lat.at[extra_unit],
+        r_lat.at[extra_unit],
+        beside,
+        jnp.logical_not(extra),
+    )
     send_weights(1)
 
-    def out_piece(j, s):
-        return out_w.at[j, s], r_out.at[j, s]
-
-    outs = (chain_out, attend_out)
+    marks_out = [[reserve(outer_n) for _ in range(inner_n)] for _ in range(2)]
     for j in range(2):
-        for d in range(1, outer_n):
-            ref, sem = out_piece(j, me)
-            launch(outs[j], ref, sem, dev(turn_o(d), i, x, k))
-        out_w[j, me] = outs[j][...]
-
-    from_lines(rec[0], 1)
-
-    def relay_unit(unit, condition=None):
-        arrive(lat.at[unit], r_lat.at[unit], condition)
-        launch(lat.at[unit], lat.at[unit], r_lat.at[unit], beside, condition)
-
-    for d in range(1, outer_n):
-        relay_unit(x * q_units + turn_o(d))
-    relay_unit(extra_unit, jnp.logical_not(extra))
+        ref, sem = out_piece(j, i, o)
+        for step, condition in ((1, right), (-1, left)):
+            launch(outs[j], ref, sem, dev(o + step, i, x, k), condition)
+        out_w[j, i, o] = outs[j][...]
+
+    def relay_out(d):
+        for j in range(2):
+
+            def act(there, valid, toward):
+                ref, sem = out_piece(j, i, there)
+                arrive(ref, sem, valid)
+                if d < outer_n - 1:
+                    onward = both(valid, right if toward > 0 else left)
+                    launch(ref, ref, sem, dev(o + toward, i, x, k), onward, marks_out[j][0] + there)
+                for e in range(1, inner_n):
+                    launch(
+                        ref, ref, sem, dev(o, turn_i(e), x, k), valid, marks_out[j][e] + there
+                    )
+
+            by_distance(d, act)
+
     from_pairs(rec[0])
-
-    for d in range(outer_n):
-        unit = (1 - x) * q_units + turn_o(d)
-        arrive(lat.at[unit], r_lat.at[unit])
-    far_unit = outer_n + 1 - x
-    arrive(lat.at[far_unit], r_lat.at[far_unit])
-
-    cosines, sines = [], []
-    for b in range(blocks):
-        s = (blocks * k + b) * inner_n + i
-        cb, sb = cos_block[pl.ds(s, 1), :], sin_block[pl.ds(s, 1), :]
-        cosines.append(cb * cos_row[...] - sb * sin_row[...])
-        sines.append(sb * cos_row[...] + cb * sin_row[...])
-    cosine = jnp.concatenate(cosines, axis=0)
-    sine = jnp.concatenate(sines, axis=0)
-
-    def latent(first_unit, count, gain):
-        wide = jnp.concatenate(
-            [lat[u].astype(f32) for u in range(first_unit, first_unit + count)], axis=1
-        )
-        return (wide * inverse_rms(wide, count * LANES) * gain[...]).astype(bf16)
-
-    def finish(plain, tail, swapped, gain):
-        square = jnp.sum(plain * plain + tail * tail, axis=-1, keepdims=True)
-        scale = lax.rsqrt(square / ATT_QK + norm_eps)
-        turned = tail * gain[:, LANES : 2 * LANES] * cosine + swapped * gain[:, 2 * LANES :] * sine
-        return jnp.concatenate(
-            [(plain * scale * gain[:, :LANES]).astype(bf16), (turned * scale).astype(bf16)], axis=1
-        )
-
-    pairs = jnp.dot(
-        latent(q_units, outer_n, latent_gain), up_l[...], preferred_element_type=f32
-    ).astype(bf16)
-    kv[i, k, :, : 2 * LANES] = finish(
-        pairs[:, :LANES].astype(f32), rotary[:, :LANES], rotary[:, LANES:], gains(key_gain)
-    )
-    kv[i, k, :, 2 * LANES :] = pairs[:, LANES:]
 
     def shared(ref, sem):
         for e in range(1, inner_n):
             launch(ref, ref, sem, dev(o, turn_i(e), x, k))
         launch(ref, ref, sem, partner)
 
-    shared(kv.at[i, k], r_kv.at[i, k])
-
-    attend_q = (
-        jnp.dot(latent(0, q_units, query_latent_gain), up_q[...], preferred_element_type=f32)
-        .astype(bf16)
-        .astype(f32)
-    )
-    query = finish(
-        attend_q[:, :LANES],
-        attend_q[:, LANES : 2 * LANES],
-        attend_q[:, 2 * LANES :],
-        gains(query_gain),
-    )
-
     def columns(s, mats_here):
-        return jnp.concatenate([w_all[s, m].reshape(depth, LANES) for m in mats_here], axis=1)
+        return jnp.concatenate([
+                w_all[lax.rem(s, inner_n), s // inner_n, m].reshape(depth, LANES)
+                for m in mats_here
+            ], axis=1)
 
     from_partner(rec[0])
     vfb = project(lambda s: columns(s, (0, 1, 2)), 3 * LANES)
@@ -544,12 +610,59 @@
     for ref, sem in state_pieces(i, k):
         shared(ref, sem)
 
-    own_line(rec[1], None, away)
-    from_lines(rec[1], 1)
-    for j in range(2):
-        ref, sem = out_piece(j, me)
-        for e in range(1, inner_n):
-            launch(outs[j], ref, sem, dev(o, turn_i(e), x, k))
+    drain(early)
+    for d in range(outer_n):
+        unit = (1 - x) * q_units + turn_o(d)
+        arrive(lat.at[unit], r_lat.at[unit])
+    far_unit = outer_n + 1 - x
+    arrive(lat.at[far_unit], r_lat.at[far_unit])
+
+    cosines, sines = [], []
+    for b in range(blocks):
+        s = (blocks * k + b) * inner_n + i
+        cb, sb = cos_block[pl.ds(s, 1), :], sin_block[pl.ds(s, 1), :]
+        cosines.append(cb * cos_row[...] - sb * sin_row[...])
+        sines.append(sb * cos_row[...] + cb * sin_row[...])
+    cosine = jnp.concatenate(cosines, axis=0)
+    sine = jnp.concatenate(sines, axis=0)
+
+    def latent(first_unit, count, gain):
+        wide = jnp.concatenate(
+            [lat[u].astype(f32) for u in range(first_unit, first_unit + count)], axis=1
+        )
+        scaling = jnp.concatenate([gain[u : u + 1] for u in range(count)], axis=1)
+        return (wide * inverse_rms(wide, count * LANES) * scaling).astype(bf16)
+
+    def finish(plain, tail, swapped, gain):
+        square = jnp.sum(plain * plain + tail * tail, axis=-1, keepdims=True)
+        scale = lax.rsqrt(square / ATT_QK + norm_eps)
+        turned = tail * gain[:, LANES : 2 * LANES] * cosine + swapped * gain[:, 2 * LANES :] * sine
+        return jnp.concatenate(
+            [(plain * scale * gain[:, :LANES]).astype(bf16), (turned * scale).astype(bf16)], axis=1
+        )
+
+    pairs = jnp.dot(
+        latent(q_units, outer_n, latent_gain), up_l[...], preferred_element_type=f32
+    ).astype(bf16)
+    kv[i, k, :, : 2 * LANES] = finish(
+        pairs[:, :LANES].astype(f32), rotary[:, :LANES], rotary[:, LANES:], gains(key_gain)
+    )
+    kv[i, k, :, 2 * LANES :] = pairs[:, LANES:]
+
+    shared(kv.at[i, k], r_kv.at[i, k])
+
+    attend_q = (
+        jnp.dot(latent(0, q_units, query_latent_gain), up_q[...], preferred_element_type=f32)
+        .astype(bf16)
+        .astype(f32)
+    )
+    query = finish(
+        attend_q[:, :LANES],
+        attend_q[:, LANES : 2 * LANES],
+        attend_q[:, 2 * LANES :],
+        gains(query_gain),
+    )
+
 
     scale = ATT_QK ** (-0.5) * 1.4426950408889634
 
@@ -563,9 +676,12 @@
         return numer, denom + jnp.sum(weight, axis=-1, keepdims=True)
 
     carry = (jnp.zeros((blocks * rows, LANES), f32), jnp.zeros((blocks * rows, 1), f32))
+    relay_out(1)
     carry = attend(carry, i, k)
     arrive(kv.at[i, other], r_kv.at[i, other])
     carry = attend(carry, i, other)
+    for d in range(1, outer_n):
+        from_line(rec[1], d)
 
     def relay_pair(ref, sem):
         arrive(ref, sem)
@@ -573,6 +689,7 @@
 
     for e in range(1, inner_n):
         relay_pair(kv.at[turn_i(e), k], r_kv.at[turn_i(e), k])
+    relay_out(2)
     for e in range(1, inner_n):
         for ref, sem in state_pieces(turn_i(e), k):
             relay_pair(ref, sem)
@@ -587,13 +704,8 @@
         rows_out * inverse_rms(rows_out, LANES) * mixer_gain_ref[:, lane(hh)]
     ).astype(bf16)
 
-    for j in range(2):
-        for d in range(1, outer_n):
-            s = turn_o(d) * inner_n + i
-            ref, sem = out_piece(j, s)
-            arrive(ref, sem)
-            for e in range(1, inner_n):
-                launch(ref, ref, sem, dev(o, turn_i(e), x, k))
+    for d in range(3, outer_n):
+        relay_out(d)
 
     from_partner(rec[1])
     qg = project(lambda s: columns(s, (3, 4)), 2 * LANES).astype(f32)
@@ -650,30 +762,50 @@
     for j in range(2):
         for e in range(1, inner_n):
             for d in range(outer_n):
-                arrive(*out_piece(j, turn_o(d) * inner_n + turn_i(e)))
+                arrive(*out_piece(j, turn_i(e), turn_o(d)))
     for h in range(heads):
         arrive(mix_recv.at[h], r_mix.at[h], heads * k + h != o)
-    chain_mixed = jnp.concatenate([mix_recv[h, :, :LANES] for h in range(heads)], axis=1)
-    attended = jnp.concatenate([mix_recv[h, :, LANES:] for h in range(heads)], axis=1)
-    col_n = out_w.shape[3]
-    for s in range(n):
-        product = jnp.dot(chain_mixed, out_w[0, s], preferred_element_type=f32) + jnp.dot(
-            attended, out_w[1, s], preferred_element_type=f32
-        )
-        for q in range(heads_n):
-            send[q, :, s * col_n : (s + 1) * col_n] = product[
-                q * part_rows : (q + 1) * part_rows
-            ].astype(bf16)
-    for d in range(1, heads_n):
-        there = lax.rem(t + d, heads_n)
-        launch(send.at[there], recv.at[d], r_sum.at[d], {"sp": me, "tp": there})
-    total = send[t].astype(f32)
-    for d in range(1, heads_n):
-        arrive(recv.at[d], r_sum.at[d])
-        total = total + recv[d].astype(f32)
-    out_ref[...] = total
-    for condition, finish_send in pending:
-        run_if(condition, finish_send)
+    col_n = out_w.shape[4]
+    spans = [range(c * n // 2, (c + 1) * n // 2) for c in range(2)]
+    own_rows = 2 * part_rows
+
+    def partial(c, x_):
+        at = pl.ds(pl.multiple_of(x_ * own_rows, own_rows), own_rows)
+        chain_part = jnp.concatenate([mix_recv[h, at, :LANES] for h in range(heads)], axis=1)
+        attend_part = jnp.concatenate([mix_recv[h, at, LANES:] for h in range(heads)], axis=1)
+        return [
+            jnp.dot(chain_part, out_w[0, s % inner_n, s // inner_n], preferred_element_type=f32)
+            + jnp.dot(attend_part, out_w[1, s % inner_n, s // inner_n], preferred_element_type=f32)
+            for s in spans[c]
+        ]
+
+    def spread_rows(target, c, x_):
+        for j, product in enumerate(partial(c, x_)):
+            at = slice(j * col_n, (j + 1) * col_n)
+            for q in range(2):
+                target[c, q, :, at] = product[q * part_rows : (q + 1) * part_rows]
+
+    for c in range(2):
+        spread_rows(part_far, c, 1 - x)
+        send_far[c] = part_far[c, other].astype(bf16)
+        launch(send_far.at[c], got_far.at[c], r_sum.at[0, c], partner)
+    for c in range(2):
+        arrive(got_far.at[c], r_sum.at[0, c])
+        send_x[c] = (part_far[c, k] + got_far[c].astype(f32)).astype(bf16)
+        launch(send_x.at[c], got_x.at[c], r_sum.at[1, c], beside)
+    for c in range(2):
+        spread_rows(part_near, c, x)
+        send_near[c] = part_near[c, other].astype(bf16)
+        launch(send_near.at[c], got_near.at[c], r_sum.at[2, c], partner)
+    for c in range(2):
+        arrive(got_near.at[c], r_sum.at[2, c])
+        arrive(got_x.at[c], r_sum.at[1, c])
+        size = len(spans[c]) * col_n
+        out_ref[:, c * size : (c + 1) * size] = (
+            part_near[c, k] + got_near[c].astype(f32) + got_x[c].astype(f32)
+        )
+    drain(len(pending))
+    needed.append(used[0])
 
 
 def on_device(
@@ -738,7 +870,7 @@
                 latent_down,
             )
         ],
-        rotary_down.reshape(n, depth, ROPE_DIM),
+        rotary_down.T,
         query_up,
         latent_up,
         chain_out,
@@ -747,28 +879,32 @@
         chain_gain[None],
         mixer_gain[None],
         input_gain[None],
-        query_latent_gain[None],
-        latent_gain[None],
+        query_latent_gain.reshape(-1, LANES),
+        latent_gain.reshape(-1, LANES),
         query_head_gain[None],
         key_head_gain[None],
         *in_row,
         *in_block,
     )
-    sends = 120 + 26 * n
     dma = pltpu.SemaphoreType.DMA
     vmem = pl.BlockSpec(memory_space=pltpu.VMEM)
     tall = blocks * rows
-    return pl.pallas_call(
-        functools.partial(mixer_kernel, n, heads_n, heads, sends),
+    needed = []
+    hbm = pl.BlockSpec(memory_space=pltpu.HBM)
+    big = operands[:13]
+
+    def build(sends):
+      return pl.pallas_call(
+        functools.partial(mixer_kernel, n, heads_n, heads, sends, needed),
         out_shape=jax.ShapeDtypeStruct((part, out_cols), f32),
-        in_specs=[vmem] * len(operands),
+        in_specs=[hbm] * len(big) + [vmem] * (len(operands) - len(big)),
         out_specs=vmem,
         scratch_shapes=[
-            pltpu.VMEM((outer_n, part, width), bf16),
+            pltpu.VMEM((2, outer_n, part, width // 2), bf16),
             pltpu.VMEM((blocks, heads_n, part, width), bf16),
             pltpu.VMEM((n, tall, depth), bf16),
-            pltpu.VMEM((n, 5, 2, half, LANES), bf16),
-            pltpu.VMEM((2, n, 2, half, LANES), bf16),
+            pltpu.VMEM((inner_n, outer_n, 5, 2, half, LANES), bf16),
+            pltpu.VMEM((2, inner_n, outer_n, 2, half, LANES), bf16),
             pltpu.VMEM((n, depth, 2 * LANES), bf16),
             pltpu.VMEM((units, tall, LANES), bf16),
             pltpu.VMEM(forget_rate.shape, f32),
@@ -781,27 +917,40 @@
             pltpu.VMEM((inner_n, outer_n, 2, 8, LANES), f32),
             pltpu.VMEM((blocks, rows, 2 * LANES), bf16),
             pltpu.VMEM((heads, rows, 2 * LANES), bf16),
-            pltpu.VMEM((2, n) + chain_out.shape, bf16),
-            pltpu.VMEM((heads_n, part, out_cols), bf16),
-            pltpu.VMEM((heads_n, part, out_cols), bf16),
+            pltpu.VMEM((2, inner_n, outer_n) + chain_out.shape, bf16),
+            pltpu.VMEM((2, 2, part, out_cols // 2), f32),
+            pltpu.VMEM((2, 2, part, out_cols // 2), f32),
+            pltpu.VMEM((2, part, out_cols // 2), bf16),
+            pltpu.VMEM((2, part, out_cols // 2), bf16),
+            pltpu.VMEM((2, part, out_cols // 2), bf16),
+            pltpu.VMEM((2, part, out_cols // 2), bf16),
+            pltpu.VMEM((2, part, out_cols // 2), bf16),
+            pltpu.VMEM((2, part, out_cols // 2), bf16),
             dma((sends,)),
-            dma((outer_n,)),
-            dma((blocks, heads_n)),
-            dma((2, n, 2)),
-            dma((2, n, 2)),
+            dma((2, outer_n)),
+            dma((2, blocks, heads_n)),
+            dma((2, inner_n, outer_n)),
+            dma((2, inner_n)),
+            dma((2, inner_n, outer_n)),
+            dma((2, inner_n)),
             dma((5,)),
             dma((units,)),
             dma((inner_n, 2)),
             dma((inner_n, 2)),
             dma((inner_n, 2)),
             dma((heads,)),
-            dma((2, n)),
-            dma((heads_n,)),
-        ],
+            dma((2, inner_n, outer_n)),
+            dma((3, 2)),
+        ]
+        + [pltpu.VMEM(a.shape, a.dtype) for a in big]
+        + [dma((len(big),))],
         compiler_params=pltpu.CompilerParams(
             collective_id=0, has_side_effects=True, vmem_limit_bytes=VMEM_LIMIT
         ),
-    )(*operands)
+      )
+
+    jax.eval_shape(build(200 + 30 * n), *operands)
+    return build(needed[0])(*operands)
 
 
 def solution(mesh):

time: 114 us -> 88.5 us (0.78)
  the two profiles are of different devices: /device:TPU:13 before, /device:TPU:0 now
where the time goes in v2:
time: 88.5 us; the launch traced here: 88.3 us
  Pallas kernels  86.6 us (98%)
  local copies, waits for them, and re-layouts  1.72 us (2%)
    pallas_call x1, Pallas kernels, on_device(): return build(needed[0])(*operands)  86.6 us

profile of v2, /device:TPU:0, one launch (start us, length us, event | category | flops | bytes accessed | tf_op | source)
XLA Modules:
  0.0 88.3 jit_solution(2438754839330165422)
XLA Ops:
  0.0 86.6 %shard_map.235 = f32[40,2048]{1,0:T(8,128)} custom-call(bf16[4,40,2048]{2,1,0:T(8,128)(2,1)} %bitcast.16, bf16[2,128,256]{2,1,0:T(8,128)(2,1)} %bitcast.20, bf16[2,128,256]{2,1,0:T(8,128)(2,1)} %bitcast.21, bf16[2,128,256]{2,1,0:T(8,128)(2,1)} %bitcast.22, bf16[2,128,256]{2,1,0:T(8,128)(2,1)} %bitcast.23, bf16[2,128,256]{2,1,0:T(8,128)(2,1)} %bitcast.24, ...), custom_call_target="tpu_custom_call" | custom-call | tf_op jit(solution)/shard_map/pallas_call | solution.py:953
  86.6 1.7 %copy.27 = f32[40,2048]{1,0:T(8,128)} copy(f32[40,2048]{1,0:T(8,128)} %shard_map.235) | data formatting | bytes 655360

commit v3 on v2

--- a/solution.py
+++ b/solution.py
@@ -9,6 +9,7 @@
 from jax.sharding import PartitionSpec as P
 
 LANES = 128
+RING = 64
 NOPE_DIM = 128
 ROPE_DIM = 64
 ATT_QK = 192
@@ -17,7 +18,7 @@
 norm_eps = 1e-06
 rope_theta = 10000.0
 MESH = pl.DeviceIdType.MESH
-VMEM_LIMIT = 60 * 1024 * 1024
+VMEM_LIMIT = 48 * 1024 * 1024
 f32 = jnp.float32
 bf16 = jnp.bfloat16
 
@@ -176,7 +177,8 @@
         pl.semaphore_signal(barrier, inc=1, device_id=peer, device_id_type=MESH)
     pl.semaphore_wait(barrier, len(peers))
 
-    pending, spare, used = [], [], [0]
+    pending, used, shared_slots = [], [0], set()
+    ring = min(sends, RING)
 
     def copy(src, dst, send_sem, recv_sem, device):
         return pltpu.make_async_remote_copy(
@@ -190,11 +192,13 @@
 
     def launch(src, dst, recv_sem, device, condition=None, index=None):
         if index is None:
-            if not spare:
-                spare.append(used[0])
+            if used[0] < ring:
+                index = used[0]
                 used[0] += 1
-            index = spare.pop(0)
-        assert used[0] <= sends
+            else:
+                at = next(a for a, entry in enumerate(pending) if entry[2] not in shared_slots)
+                finished, finish_send, index = pending.pop(at)
+                run_if(finished, finish_send)
 
         def make():
             return copy(src, dst, ssem.at[index], recv_sem, device)
@@ -202,23 +206,15 @@
         run_if(condition, lambda: make().start())
         pending.append((condition, lambda: make().wait_send(), index))
         return index
-
-    def reserve(size):
-        base = used[0]
-        used[0] += size
-        return base
 
     def by_distance(d, act):
         for there, toward in ((o - d, 1), (o + d, -1)):
             valid = (there >= 0) & (there < outer_n)
             act(jnp.clip(there, 0, outer_n - 1), valid, toward)
 
-    def drain(first):
-        for condition, finish_send, index in pending[:first]:
+    def drain():
+        for condition, finish_send, _ in pending:
             run_if(condition, finish_send)
-            if isinstance(index, int) and index not in spare:
-                spare.append(index)
-        del pending[:first]
 
     def arrive(dst, recv_sem, condition=None):
         run_if(
@@ -258,6 +254,7 @@
                 condition,
                 index,
             )
+        shared_slots.add(index)
     launch(
         q_down.at[k, :, lane(extra_unit)],
         l_all.at[1, i, o, k],
@@ -359,7 +356,7 @@
             ref, sem = piece[0](i, there)
             arrive(ref, sem, valid)
             for e in range(1, inner_n):
-                launch(ref, ref, sem, dev(o, turn_i(e), x, k), valid, piece[2][e] + there)
+                launch(ref, ref, sem, dev(o, turn_i(e), x, k), valid)
 
         by_distance(d, act)
         if d == outer_n - 1:
@@ -380,8 +377,7 @@
             arrive(*piece[1](turn_i(e), other), condition)
 
     def kind(piece, block, which):
-        marks = [reserve(outer_n) for _ in range(inner_n)]
-        return functools.partial(piece, which), functools.partial(block, which), marks
+        return functools.partial(piece, which), functools.partial(block, which)
 
     lat_a, lat_b = kind(lat_piece, lat_block, 0), kind(lat_piece, lat_block, 1)
     rec = [kind(rec_piece, rec_block, g) for g in range(2)]
@@ -427,19 +423,43 @@
         preferred_element_type=f32,
     ).astype(bf16)
 
-    marks = [[reserve(outer_n) for _ in range(3)] for _ in range(2)]
+    for j in range(2):
+        out_w[j, i, o] = outs[j][...]
+
+    def send_out(js=(0, 1)):
+        for j in js:
+            ref, sem = out_piece(j, i, o)
+            for step, condition in ((1, right), (-1, left)):
+                launch(outs[j], ref, sem, dev(o + step, i, x, k), condition)
+
+    def relay_out(d, js=(0, 1)):
+        for j in js:
+
+            def act(there, valid, toward):
+                ref, sem = out_piece(j, i, there)
+                arrive(ref, sem, valid)
+                if d < outer_n - 1:
+                    onward = both(valid, right if toward > 0 else left)
+                    launch(ref, ref, sem, dev(o + toward, i, x, k), onward)
+                for e in range(1, inner_n):
+                    launch(
+                        ref, ref, sem, dev(o, turn_i(e), x, k), valid
+                    )
+
+            by_distance(d, act)
+
 
     def relay_tokens(c, there, valid, toward, last):
         ref, sem = stage.at[c, there], r_tok.at[c, there]
         arrive(ref, sem, valid)
         if not last:
             onward = both(valid, right if toward > 0 else left)
-            launch(ref, ref, sem, dev(o + toward, i, x, k), onward, marks[c][0] + there)
+            launch(ref, ref, sem, dev(o + toward, i, x, k), onward)
         core, b = there // blocks, lax.rem(there, blocks)
         at = halves[c]
         target, sem = tok.at[b, t, :, at], r_deliver.at[c, b, t]
-        launch(ref, target, sem, dev(o, i, 1 - x, core), valid, marks[c][1] + there)
-        launch(ref, target, sem, partner, both(valid, core != k), marks[c][2] + there)
+        launch(ref, target, sem, dev(o, i, 1 - x, core), valid)
+        launch(ref, target, sem, partner, both(valid, core != k))
 
         @pl.when(both(valid, core == k))
         def _():
@@ -507,18 +527,17 @@
             launch(lat.at[unit], lat.at[unit], r_lat.at[unit], dev(turn_o(d), i, x, k), condition)
         launch(lat.at[unit], lat.at[unit], r_lat.at[unit], beside, condition)
 
-    early = len(pending)
     send_unit(own_unit)
     send_unit(extra_unit, extra)
+    send_out((0,))
     for d in range(1, outer_n):
         from_line(rec[0], d)
 
-    marks_x = reserve(outer_n)
 
     def relay_unit(there, valid, toward):
         unit = x * q_units + there
         arrive(lat.at[unit], r_lat.at[unit], valid)
-        launch(lat.at[unit], lat.at[unit], r_lat.at[unit], beside, valid, marks_x + there)
+        launch(lat.at[unit], lat.at[unit], r_lat.at[unit], beside, valid)
 
     for d in range(1, outer_n):
         by_distance(d, relay_unit)
@@ -531,31 +550,9 @@
         jnp.logical_not(extra),
     )
     send_weights(1)
-
-    marks_out = [[reserve(outer_n) for _ in range(inner_n)] for _ in range(2)]
-    for j in range(2):
-        ref, sem = out_piece(j, i, o)
-        for step, condition in ((1, right), (-1, left)):
-            launch(outs[j], ref, sem, dev(o + step, i, x, k), condition)
-        out_w[j, i, o] = outs[j][...]
-
-    def relay_out(d):
-        for j in range(2):
-
-            def act(there, valid, toward):
-                ref, sem = out_piece(j, i, there)
-                arrive(ref, sem, valid)
-                if d < outer_n - 1:
-                    onward = both(valid, right if toward > 0 else left)
-                    launch(ref, ref, sem, dev(o + toward, i, x, k), onward, marks_out[j][0] + there)
-                for e in range(1, inner_n):
-                    launch(
-                        ref, ref, sem, dev(o, turn_i(e), x, k), valid, marks_out[j][e] + there
-                    )
-
-            by_distance(d, act)
-
+    send_out((1,))
     from_pairs(rec[0])
+    relay_out(1, (0,))
 
     def shared(ref, sem):
         for e in range(1, inner_n):
@@ -610,7 +607,6 @@
     for ref, sem in state_pieces(i, k):
         shared(ref, sem)
 
-    drain(early)
     for d in range(outer_n):
         unit = (1 - x) * q_units + turn_o(d)
         arrive(lat.at[unit], r_lat.at[unit])
@@ -676,12 +672,13 @@
         return numer, denom + jnp.sum(weight, axis=-1, keepdims=True)
 
     carry = (jnp.zeros((blocks * rows, LANES), f32), jnp.zeros((blocks * rows, 1), f32))
-    relay_out(1)
     carry = attend(carry, i, k)
     arrive(kv.at[i, other], r_kv.at[i, other])
     carry = attend(carry, i, other)
     for d in range(1, outer_n):
         from_line(rec[1], d)
+    relay_out(1, (1,))
+    relay_out(2, (0,))
 
     def relay_pair(ref, sem):
         arrive(ref, sem)
@@ -689,11 +686,12 @@
 
     for e in range(1, inner_n):
         relay_pair(kv.at[turn_i(e), k], r_kv.at[turn_i(e), k])
-    relay_out(2)
     for e in range(1, inner_n):
         for ref, sem in state_pieces(turn_i(e), k):
             relay_pair(ref, sem)
     from_pairs(rec[1])
+    relay_out(2, (1,))
+    relay_out(3, (0,))
     for e in range(1, inner_n):
         there = turn_i(e)
         carry = attend(carry, there, k)
@@ -703,9 +701,6 @@
     attend_mixed = (
         rows_out * inverse_rms(rows_out, LANES) * mixer_gain_ref[:, lane(hh)]
     ).astype(bf16)
-
-    for d in range(3, outer_n):
-        relay_out(d)
 
     from_partner(rec[1])
     qg = project(lambda s: columns(s, (3, 4)), 2 * LANES).astype(f32)
@@ -759,52 +754,61 @@
         def _():
             mix_recv[hh] = mix_send[b]
 
-    for j in range(2):
-        for e in range(1, inner_n):
-            for d in range(outer_n):
-                arrive(*out_piece(j, turn_i(e), turn_o(d)))
+    relay_out(3, (1,))
+
     for h in range(heads):
         arrive(mix_recv.at[h], r_mix.at[h], heads * k + h != o)
     col_n = out_w.shape[4]
-    spans = [range(c * n // 2, (c + 1) * n // 2) for c in range(2)]
+    span = inner_n * col_n
     own_rows = 2 * part_rows
-
-    def partial(c, x_):
+    order = (o, o + 1 - 2 * lax.rem(o, 2), turn_o(2), outer_n - 1 - o)
+    assert outer_n == len(order)
+
+    def rows_of(x_):
         at = pl.ds(pl.multiple_of(x_ * own_rows, own_rows), own_rows)
-        chain_part = jnp.concatenate([mix_recv[h, at, :LANES] for h in range(heads)], axis=1)
-        attend_part = jnp.concatenate([mix_recv[h, at, LANES:] for h in range(heads)], axis=1)
         return [
-            jnp.dot(chain_part, out_w[0, s % inner_n, s // inner_n], preferred_element_type=f32)
-            + jnp.dot(attend_part, out_w[1, s % inner_n, s // inner_n], preferred_element_type=f32)
-            for s in spans[c]
+            jnp.concatenate(
+                [mix_recv[h, at, p * LANES : (p + 1) * LANES] for h in range(heads)], axis=1
+            )
+            for p in range(2)
         ]
 
-    def spread_rows(target, c, x_):
-        for j, product in enumerate(partial(c, x_)):
-            at = slice(j * col_n, (j + 1) * col_n)
+    def partial(target, c, rows_here):
+        for e in range(inner_n):
+            product = jnp.dot(
+                rows_here[0], out_w[0, e, order[c]], preferred_element_type=f32
+            ) + jnp.dot(rows_here[1], out_w[1, e, order[c]], preferred_element_type=f32)
             for q in range(2):
-                target[c, q, :, at] = product[q * part_rows : (q + 1) * part_rows]
-
-    for c in range(2):
-        spread_rows(part_far, c, 1 - x)
-        send_far[c] = part_far[c, other].astype(bf16)
-        launch(send_far.at[c], got_far.at[c], r_sum.at[0, c], partner)
-    for c in range(2):
+                target[c, q, :, e * col_n : (e + 1) * col_n] = product[
+                    q * part_rows : (q + 1) * part_rows
+                ]
+
+    rows_far, rows_near = rows_of(1 - x), rows_of(x)
+    def cross(c):
         arrive(got_far.at[c], r_sum.at[0, c])
         send_x[c] = (part_far[c, k] + got_far[c].astype(f32)).astype(bf16)
         launch(send_x.at[c], got_x.at[c], r_sum.at[1, c], beside)
-    for c in range(2):
-        spread_rows(part_near, c, x)
+
+    for c in range(outer_n):
+        for j in range(2):
+            for e in range(1, inner_n):
+                arrive(*out_piece(j, turn_i(e), order[c]))
+        partial(part_far, c, rows_far)
+        send_far[c] = part_far[c, other].astype(bf16)
+        launch(send_far.at[c], got_far.at[c], r_sum.at[0, c], partner)
+        if c:
+            cross(c - 1)
+        partial(part_near, c, rows_near)
         send_near[c] = part_near[c, other].astype(bf16)
         launch(send_near.at[c], got_near.at[c], r_sum.at[2, c], partner)
-    for c in range(2):
+    cross(outer_n - 1)
+    for c in range(outer_n):
         arrive(got_near.at[c], r_sum.at[2, c])
         arrive(got_x.at[c], r_sum.at[1, c])
-        size = len(spans[c]) * col_n
-        out_ref[:, c * size : (c + 1) * size] = (
+        out_ref[:, lane(order[c], span)] = (
             part_near[c, k] + got_near[c].astype(f32) + got_x[c].astype(f32)
         )
-    drain(len(pending))
+    drain()
     needed.append(used[0])
 
 
@@ -918,14 +922,14 @@
             pltpu.VMEM((blocks, rows, 2 * LANES), bf16),
             pltpu.VMEM((heads, rows, 2 * LANES), bf16),
             pltpu.VMEM((2, inner_n, outer_n) + chain_out.shape, bf16),
-            pltpu.VMEM((2, 2, part, out_cols // 2), f32),
-            pltpu.VMEM((2, 2, part, out_cols // 2), f32),
-            pltpu.VMEM((2, part, out_cols // 2), bf16),
-            pltpu.VMEM((2, part, out_cols // 2), bf16),
-            pltpu.VMEM((2, part, out_cols // 2), bf16),
-            pltpu.VMEM((2, part, out_cols // 2), bf16),
-            pltpu.VMEM((2, part, out_cols // 2), bf16),
-            pltpu.VMEM((2, part, out_cols // 2), bf16),
+            pltpu.VMEM((outer_n, 2, part, out_cols // outer_n), f32),
+            pltpu.VMEM((outer_n, 2, part, out_cols // outer_n), f32),
+            pltpu.VMEM((outer_n, part, out_cols // outer_n), bf16),
+            pltpu.VMEM((outer_n, part, out_cols // outer_n), bf16),
+            pltpu.VMEM((outer_n, part, out_cols // outer_n), bf16),
+            pltpu.VMEM((outer_n, part, out_cols // outer_n), bf16),
+            pltpu.VMEM((outer_n, part, out_cols // outer_n), bf16),
+            pltpu.VMEM((outer_n, part, out_cols // outer_n), bf16),
             dma((sends,)),
             dma((2, outer_n)),
             dma((2, blocks, heads_n)),
@@ -940,7 +944,7 @@
             dma((inner_n, 2)),
             dma((heads,)),
             dma((2, inner_n, outer_n)),
-            dma((3, 2)),
+            dma((3, outer_n)),
         ]
         + [pltpu.VMEM(a.shape, a.dtype) for a in big]
         + [dma((len(big),))],
@@ -950,7 +954,8 @@
       )
 
     jax.eval_shape(build(200 + 30 * n), *operands)
-    return build(needed[0])(*operands)
+    held = [pltpu.with_memory_space_constraint(a, pltpu.HBM) for a in operands]
+    return build(needed[0])(*held)
 
 
 def solution(mesh):

time: 88.5 us -> 80.4 us (0.908)
  the two profiles are of different devices: /device:TPU:0 before, /device:TPU:13 now
where the time goes in v3:
time: 80.4 us; the launch traced here: 80.2 us
  Pallas kernels  79.5 us (99%)
    pallas_call x1, Pallas kernels, on_device(): return build(needed[0])(*held)  79.5 us

profile of v3, /device:TPU:13, one launch (start us, length us, event | category | flops | bytes accessed | tf_op | source)
XLA Modules:
  0.0 80.2 jit_solution(304371746217209985)
XLA Ops:
  0.0 79.5 %shard_map.235 = f32[40,2048]{1,0:T(8,128)S(1)} custom-call(bf16[4,40,2048]{2,1,0:T(8,128)(2,1)} %bitcast.16, bf16[2,128,256]{2,1,0:T(8,128)(2,1)} %bitcast.20, bf16[2,128,256]{2,1,0:T(8,128)(2,1)} %bitcast.21, bf16[2,128,256]{2,1,0:T(8,128)(2,1)} %bitcast.22, bf16[2,128,256]{2,1,0:T(8,128)(2,1)} %bitcast.23, bf16[2,128,256]{2,1,0:T(8,128)(2,1)} %bitcast.24, ...), custom_call_target="tpu_custom_call" | custom-call | tf_op jit(solution)/shard_map/pallas_call | solution.py:958
  79.5 0.7 copy.27

commit v4 on v3

--- a/solution.py
+++ b/solution.py
@@ -633,17 +633,23 @@
         square = jnp.sum(plain * plain + tail * tail, axis=-1, keepdims=True)
         scale = lax.rsqrt(square / ATT_QK + norm_eps)
         turned = tail * gain[:, LANES : 2 * LANES] * cosine + swapped * gain[:, 2 * LANES :] * sine
-        return jnp.concatenate(
-            [(plain * scale * gain[:, :LANES]).astype(bf16), (turned * scale).astype(bf16)], axis=1
-        )
+        return (plain * scale * gain[:, :LANES]).astype(bf16), turned * scale
 
     pairs = jnp.dot(
         latent(q_units, outer_n, latent_gain), up_l[...], preferred_element_type=f32
     ).astype(bf16)
-    kv[i, k, :, : 2 * LANES] = finish(
+    key_plain, key_turned = finish(
         pairs[:, :LANES].astype(f32), rotary[:, :LANES], rotary[:, LANES:], gains(key_gain)
     )
-    kv[i, k, :, 2 * LANES :] = pairs[:, LANES:]
+    assert blocks * ROPE_DIM == LANES
+    packed = jnp.zeros((rows, LANES), f32)
+    for b in range(blocks):
+        at = slice(b * rows, (b + 1) * rows)
+        kv[i, k, b] = key_plain[at]
+        kv[i, k, blocks + b] = pairs[at, LANES:]
+        part = key_turned[at]
+        packed += pltpu.roll(part, b * ROPE_DIM, axis=1) if b else part
+    kv[i, k, 2 * blocks] = packed.astype(bf16)
 
     shared(kv.at[i, k], r_kv.at[i, k])
 
@@ -652,24 +658,36 @@
         .astype(bf16)
         .astype(f32)
     )
-    query = finish(
+    query_plain, query_turned = finish(
         attend_q[:, :LANES],
         attend_q[:, LANES : 2 * LANES],
         attend_q[:, 2 * LANES :],
         gains(query_gain),
     )
+    queries = [
+        jnp.concatenate(
+            [
+                query_plain,
+                (pltpu.roll(query_turned, b * ROPE_DIM, axis=1) if b else query_turned).astype(bf16),
+            ],
+            axis=1,
+        )
+        for b in range(blocks)
+    ]
 
 
     scale = ATT_QK ** (-0.5) * 1.4426950408889634
 
     def attend(carry, i_, k_):
         numer, denom = carry
-        score = against(query, kv[i_, k_, :, : 2 * LANES])
-        weight = jnp.exp2(score * scale)
-        numer += jnp.dot(
-            weight.astype(bf16), kv[i_, k_, :, 2 * LANES :], preferred_element_type=f32
-        )
-        return numer, denom + jnp.sum(weight, axis=-1, keepdims=True)
+        for b in range(blocks):
+            key = jnp.concatenate([kv[i_, k_, b], kv[i_, k_, 2 * blocks]], axis=1)
+            weight = jnp.exp2(against(queries[b], key) * scale)
+            numer += jnp.dot(
+                weight.astype(bf16), kv[i_, k_, blocks + b], preferred_element_type=f32
+            )
+            denom += jnp.sum(weight, axis=-1, keepdims=True)
+        return numer, denom
 
     carry = (jnp.zeros((blocks * rows, LANES), f32), jnp.zeros((blocks * rows, 1), f32))
     carry = attend(carry, i, k)
@@ -689,9 +707,9 @@
     for e in range(1, inner_n):
         for ref, sem in state_pieces(turn_i(e), k):
             relay_pair(ref, sem)
-    from_pairs(rec[1])
     relay_out(2, (1,))
     relay_out(3, (0,))
+    from_pairs(rec[1])
     for e in range(1, inner_n):
         there = turn_i(e)
         carry = attend(carry, there, k)
@@ -701,6 +719,25 @@
     attend_mixed = (
         rows_out * inverse_rms(rows_out, LANES) * mixer_gain_ref[:, lane(hh)]
     ).astype(bf16)
+
+    def send_mix(p):
+        for b in range(blocks):
+            home = blocks * k + b == o
+            launch(
+                mix_send.at[p, b],
+                mix_recv.at[p, hh],
+                r_mix.at[p, hh],
+                dev(blocks * k + b, i, x, o // heads),
+                jnp.logical_not(home),
+            )
+
+            @pl.when(home)
+            def _():
+                mix_recv[p, hh] = mix_send[p, b]
+
+    for b in range(blocks):
+        mix_send[1, b] = attend_mixed[b * rows : (b + 1) * rows]
+    send_mix(1)
 
     from_partner(rec[1])
     qg = project(lambda s: columns(s, (3, 4)), 2 * LANES).astype(f32)
@@ -739,51 +776,48 @@
         total += jnp.dot(within.astype(bf16), value[b], preferred_element_type=f32)
         gate = qg[at, LANES:]
         scaled = total * inverse_rms(total, LANES) * chain_gain_ref[:, lane(hh)]
-        mix_send[b, :, :LANES] = (scaled * (gate * jax.nn.sigmoid(gate))).astype(bf16)
-        mix_send[b, :, LANES:] = attend_mixed[at]
-        home = there == o
-        launch(
-            mix_send.at[b],
-            mix_recv.at[hh],
-            r_mix.at[hh],
-            dev(there, i, x, o // heads),
-            jnp.logical_not(home),
-        )
-
-        @pl.when(home)
-        def _():
-            mix_recv[hh] = mix_send[b]
-
+        mix_send[0, b] = (scaled * (gate * jax.nn.sigmoid(gate))).astype(bf16)
+    send_mix(0)
     relay_out(3, (1,))
 
     for h in range(heads):
-        arrive(mix_recv.at[h], r_mix.at[h], heads * k + h != o)
+        for p in range(2):
+            arrive(mix_recv.at[p, h], r_mix.at[p, h], heads * k + h != o)
     col_n = out_w.shape[4]
     span = inner_n * col_n
     own_rows = 2 * part_rows
     order = (o, o + 1 - 2 * lax.rem(o, 2), turn_o(2), outer_n - 1 - o)
     assert outer_n == len(order)
 
-    def rows_of(x_):
-        at = pl.ds(pl.multiple_of(x_ * own_rows, own_rows), own_rows)
-        return [
-            jnp.concatenate(
-                [mix_recv[h, at, p * LANES : (p + 1) * LANES] for h in range(heads)], axis=1
-            )
-            for p in range(2)
-        ]
-
-    def partial(target, c, rows_here):
+    def rows_of(p):
+        return jnp.concatenate(
+            [
+                jnp.concatenate(
+                    [
+                        mix_recv[p, h, pl.ds(pl.multiple_of(x_ * own_rows, own_rows), own_rows), :]
+                        for h in range(heads)
+                    ],
+                    axis=1,
+                )
+                for x_ in (1 - x, x)
+            ],
+            axis=0,
+        )
+
+    def partial(c):
         for e in range(inner_n):
             product = jnp.dot(
-                rows_here[0], out_w[0, e, order[c]], preferred_element_type=f32
-            ) + jnp.dot(rows_here[1], out_w[1, e, order[c]], preferred_element_type=f32)
-            for q in range(2):
-                target[c, q, :, e * col_n : (e + 1) * col_n] = product[
-                    q * part_rows : (q + 1) * part_rows
-                ]
-
-    rows_far, rows_near = rows_of(1 - x), rows_of(x)
+                all_rows[0], out_w[0, e, order[c]], preferred_element_type=f32
+            ) + jnp.dot(all_rows[1], out_w[1, e, order[c]], preferred_element_type=f32)
+            for side, target in enumerate((part_far, part_near)):
+                for q in range(2):
+                    first_row = side * own_rows + q * part_rows
+                    target[c, q, :, e * col_n : (e + 1) * col_n] = product[
+                        first_row : first_row + part_rows
+                    ]
+
+    all_rows = [rows_of(p) for p in range(2)]
+
     def cross(c):
         arrive(got_far.at[c], r_sum.at[0, c])
         send_x[c] = (part_far[c, k] + got_far[c].astype(f32)).astype(bf16)
@@ -793,14 +827,13 @@
         for j in range(2):
             for e in range(1, inner_n):
                 arrive(*out_piece(j, turn_i(e), order[c]))
-        partial(part_far, c, rows_far)
+        partial(c)
         send_far[c] = part_far[c, other].astype(bf16)
         launch(send_far.at[c], got_far.at[c], r_sum.at[0, c], partner)
+        send_near[c] = part_near[c, other].astype(bf16)
+        launch(send_near.at[c], got_near.at[c], r_sum.at[2, c], partner)
         if c:
             cross(c - 1)
-        partial(part_near, c, rows_near)
-        send_near[c] = part_near[c, other].astype(bf16)
-        launch(send_near.at[c], got_near.at[c], r_sum.at[2, c], partner)
     cross(outer_n - 1)
     for c in range(outer_n):
         arrive(got_near.at[c], r_sum.at[2, c])
@@ -916,11 +949,11 @@
             pltpu.VMEM((1,) + mixer_gain.shape, f32),
             pltpu.VMEM(query_up.shape, bf16),
             pltpu.VMEM((latent_up.shape[0], 2 * LANES), bf16),
-            pltpu.VMEM((inner_n, 2, tall, 3 * LANES), bf16),
+            pltpu.VMEM((inner_n, 2, 2 * blocks + 1, rows, LANES), bf16),
             pltpu.VMEM((inner_n, outer_n, 2, LANES, LANES), bf16),
             pltpu.VMEM((inner_n, outer_n, 2, 8, LANES), f32),
-            pltpu.VMEM((blocks, rows, 2 * LANES), bf16),
-            pltpu.VMEM((heads, rows, 2 * LANES), bf16),
+            pltpu.VMEM((2, blocks, rows, LANES), bf16),
+            pltpu.VMEM((2, heads, rows, LANES), bf16),
             pltpu.VMEM((2, inner_n, outer_n) + chain_out.shape, bf16),
             pltpu.VMEM((outer_n, 2, part, out_cols // outer_n), f32),
             pltpu.VMEM((outer_n, 2, part, out_cols // outer_n), f32),
@@ -942,7 +975,7 @@
             dma((inner_n, 2)),
             dma((inner_n, 2)),
             dma((inner_n, 2)),
-            dma((heads,)),
+            dma((2, heads)),
             dma((2, inner_n, outer_n)),
             dma((3, outer_n)),
         ]

time: 80.4 us -> 79.6 us (0.990)
    pallas_call x1, Pallas kernels: 79.5 us -> 78.7 us  [on_device(): return build(needed[0])(*held)]
where the time goes in v4:
time: 79.6 us; the launch traced here: 79.4 us
  Pallas kernels  78.7 us (99%)
    pallas_call x1, Pallas kernels, on_device(): return build(needed[0])(*held)  78.7 us

profile of v4, /device:TPU:13, one launch (start us, length us, event | category | flops | bytes accessed | tf_op | source)
XLA Modules:
  0.0 79.4 jit_solution(2005290164320347704)
XLA Ops:
  0.0 78.7 %shard_map.235 = f32[40,2048]{1,0:T(8,128)S(1)} custom-call(bf16[4,40,2048]{2,1,0:T(8,128)(2,1)} %bitcast.16, bf16[2,128,256]{2,1,0:T(8,128)(2,1)} %bitcast.20, bf16[2,128,256]{2,1,0:T(8,128)(2,1)} %bitcast.21, bf16[2,128,256]{2,1,0:T(8,128)(2,1)} %bitcast.22, bf16[2,128,256]{2,1,0:T(8,128)(2,1)} %bitcast.23, bf16[2,128,256]{2,1,0:T(8,128)(2,1)} %bitcast.24, ...), custom_call_target="tpu_custom_call" | custom-call | tf_op jit(solution)/shard_map/pallas_call | solution.py:991
  78.7 0.7 copy.27

commit v5 on v4

--- a/solution.py
+++ b/solution.py
@@ -9,7 +9,7 @@
 from jax.sharding import PartitionSpec as P
 
 LANES = 128
-RING = 64
+RING = 54
 NOPE_DIM = 128
 ROPE_DIM = 64
 ATT_QK = 192
@@ -62,8 +62,7 @@
 
 def mixer_kernel(n, heads_n, heads, sends, needed, *refs):
     count = 13
-    far, near_by = refs[:count], refs[-count - 1 : -1]
-    fetched = refs[-1]
+    far, near_by = refs[:count], refs[-count:]
     (
         tok_in,
         wv,
@@ -134,7 +133,7 @@
         r_mix,
         r_out,
         r_sum,
-    ) = refs[count : -count - 1]
+    ) = refs[count:-count]
     mats = (wv, wf, wb, wq, wg)
     groups = ((0, 3), (3, 2))
     outer_n = 2 * heads
@@ -169,7 +168,7 @@
     peers = [dev(turn_o(d), i, x, r) for d in range(1, outer_n) for r in range(2)]
     peers += [dev(o, turn_i(d), x, k) for d in range(1, inner_n)]
     peers += [{"sp": me, "tp": lax.rem(t + d, heads_n)} for d in range(1, heads_n)]
-    fetches = [pltpu.make_async_copy(far[j], near_by[j], fetched.at[j]) for j in range(count)]
+    fetches = [pltpu.make_async_copy(far[j], near_by[j], ssem.at[min(sends, RING) - 1 - j]) for j in range(count)]
     for fetch in fetches:
         fetch.start()
     barrier = pltpu.get_barrier_semaphore()
@@ -979,8 +978,7 @@
             dma((2, inner_n, outer_n)),
             dma((3, outer_n)),
         ]
-        + [pltpu.VMEM(a.shape, a.dtype) for a in big]
-        + [dma((len(big),))],
+        + [pltpu.VMEM(a.shape, a.dtype) for a in big],
         compiler_params=pltpu.CompilerParams(
             collective_id=0, has_side_effects=True, vmem_limit_bytes=VMEM_LIMIT
         ),

time: 79.6 us -> 79.4 us (level)
  no operation moved by 1% of the time
where the time goes in v5:
time: 79.4 us; the launch traced here: 79.2 us
  Pallas kernels  78.5 us (99%)
    pallas_call x1, Pallas kernels, on_device(): return build(needed[0])(*held)  78.5 us

profile of v5, /device:TPU:13, one launch (start us, length us, event | category | flops | bytes accessed | tf_op | source)
XLA Modules:
  0.0 79.2 jit_solution(3194132015128395759)
XLA Ops:
  0.0 78.5 %shard_map.235 = f32[40,2048]{1,0:T(8,128)S(1)} custom-call(bf16[4,40,2048]{2,1,0:T(8,128)(2,1)} %bitcast.16, bf16[2,128,256]{2,1,0:T(8,128)(2,1)} %bitcast.20, bf16[2,128,256]{2,1,0:T(8,128)(2,1)} %bitcast.21, bf16[2,128,256]{2,1,0:T(8,128)(2,1)} %bitcast.22, bf16[2,128,256]{2,1,0:T(8,128)(2,1)} %bitcast.23, bf16[2,128,256]{2,1,0:T(8,128)(2,1)} %bitcast.24, ...), custom_call_target="tpu_custom_call" | custom-call | tf_op jit(solution)/shard_map/pallas_call | solution.py:989
  78.5 0.7 copy.27
